TPU v7x, 32 devices: a whole 2x2x4 slice. The times are simulated.
32 devices in a mesh: fs: 16 (over z, y, x), tp: 2 (over core).
Axes of the slice: x: 2, y: 2, z: 4, core: 2. Of those that a mesh axis runs over, the one named last changes fastest.
Arguments:
- inputs: bfloat16 [8192, 2048], P('fs', 'tp'), may hold values from -6 to 6
- hidden_pre: bfloat16 [8192, 4096], P('fs', 'tp'), may hold values from -6 to 6
- norm_input: bfloat16 [8192, 2048], P('fs', 'tp'), may hold values from -48 to 48, as said below
- out_gain: float32 [2048], P('tp'), may hold values from 0.1 to 1.9
- w_up: bfloat16 [2048, 4096], P('tp', 'fs'), may hold values from -0.125 to 0.125
- w_down: bfloat16 [4096, 2048], P('tp', 'fs'), may hold values from -0.09375 to 0.09375
- cotangent: bfloat16 [8192, 2048], P('fs', 'tp'), may hold values from -6 to 6
Outputs:
- grad_input: bfloat16 [8192, 2048], P('fs', 'tp')
- grad_up: float32 [2048, 4096], P('tp', 'fs')
- grad_gain: float32 [2048], P('tp')
Inputs may be any that keep to these rules, and one draw needn't show every extreme that they name: `norm_input`: each token's features are scaled by a factor of that token, and each block of 2048 / 2 features by a factor of that block.
All inputs are finite; a program needn't handle non-finite values.
Results may differ from a plain program's by a relative error of at most 0.0058.
Values may be sent and summed in bfloat16 or wider, within the bound.
A program may use at most 64 MiB of HBM per device.

v0:
```python
import functools

import jax
import jax.numpy as jnp
from jax import lax
from jax.experimental import pallas as pl
from jax.experimental.pallas import tpu as pltpu
from jax.sharding import PartitionSpec as P


norm_eps = 1e-06
MESH = pl.DeviceIdType.MESH
SEMS = 256


def trade(x, axis, mask):
    if mask == 0:
        return x
    return lax.ppermute(x, axis, [(i, i ^ mask) for i in range(lax.axis_size(axis))])


def total(x, axis):
    step = 1
    while step < lax.axis_size(axis):
        x = x + trade(x, axis, step)
        step *= 2
    return x


def masks_of(n):
    masks = [1 << i for i in range(n.bit_length() - 1)]
    return (masks, masks[::-1])


def halves(x):
    rows = x.shape[0] // 2
    return (x[:rows], x[rows:])


def gather_near(x, near_n):
    parts = []
    for part, masks in zip(halves(x), masks_of(near_n)):
        held = {0: part}
        for mask in masks:
            held.update({k ^ mask: trade(v, "fs", mask) for k, v in list(held.items())})
        parts.append(held)
    return parts


def scatter_near(pieces, near_n):
    sums = []
    for side, masks in enumerate(masks_of(near_n)):
        held = {k: halves(v)[side] for k, v in pieces.items()}
        for mask in masks:
            sent = {k: held.pop(k) for k in list(held) if k & mask}
            for k, v in sent.items():
                came = trade(v.astype(jnp.bfloat16), "fs", mask).astype(jnp.float32)
                held[k ^ mask] = held[k ^ mask] + came
        sums.append(held[0])
    return jnp.concatenate(sums, axis=0)


def tree(x, n, unit):
    terms = [trade(x, "fs", k * unit) for k in range(n)]
    while len(terms) > 1:
        terms = [a + b for a, b in zip(terms[::2], terms[1::2])]
    return terms[0]


def pick(stack, index):
    return lax.dynamic_index_in_dim(stack, index, 0, keepdims=False)


def dot(a, b, dim):
    return lax.dot_general(
        a, b, (((dim,), (dim,)), ((), ())), preferred_element_type=jnp.float32
    )


def on_device(inputs, hidden_pre, norm_input, out_gain, w_up, w_down, cotangent):
    fs, tp = lax.axis_size("fs"), lax.axis_size("tp")
    near_n = 1
    while 4 * near_n * near_n <= fs:
        near_n *= 2
    far_n = fs // near_n
    per = far_n // tp
    me, core = lax.axis_index("fs"), lax.axis_index("tp")
    far, near = me // near_n, me % near_n
    rows = inputs.shape[0]
    width = inputs.shape[1] * tp
    scaled = (rows * fs) ** (-0.5)
    block = w_up.shape[1]
    cols = w_down.shape[1]

    down_rows = w_down.reshape(per, near_n, block, cols)
    asked = [
        lax.dynamic_index_in_dim(down_rows, near ^ k, 1, keepdims=False).reshape(per * block, cols)
        for k in range(near_n)
    ]
    arrived = [trade(x, "fs", k) for k, x in enumerate(asked)]
    arrived = jnp.stack(arrived)
    down_near = jnp.concatenate([pick(arrived, near ^ i) for i in range(near_n)], axis=1)
    down_far = [trade(down_near, "fs", k * near_n) for k in range(far_n)]
    up_far = [trade(w_up, "fs", k * near_n) for k in range(far_n)]
    up_far = jnp.stack(up_far)
    down_far = jnp.stack(down_far)
    down, up = [], []
    for t in range(tp):
        places = [((core ^ t) * per + j) ^ far for j in range(per)]
        down.append(jnp.concatenate([pick(down_far, i) for i in places], axis=1))
        up.append(jnp.concatenate([pick(up_far, i) for i in places], axis=1))

    asked = [
        jnp.concatenate(
            [
                lax.dynamic_slice_in_dim(
                    hidden_pre, (j * near_n + (near ^ k)) * block, block, axis=1
                )
                for j in range(per)
            ],
            axis=1,
        )
        for k in range(near_n)
    ]
    pre = [trade(x, "fs", k) for k, x in enumerate(asked)]

    normed = norm_input.astype(jnp.float32)
    upstream = cotangent.astype(jnp.float32)
    weighted = upstream * out_gain
    sums = total(
        jnp.stack([jnp.sum(normed * normed, axis=1), jnp.sum(weighted * normed, axis=1)]), "tp"
    )
    inv_rms = lax.rsqrt(sums[0] / width + norm_eps)[:, None]
    cross_mean = (sums[1] / width)[:, None]
    d_out = (weighted * inv_rms - normed * inv_rms * inv_rms * inv_rms * cross_mean).astype(
        jnp.bfloat16
    )
    gain = jnp.sum(upstream * normed * inv_rms, axis=0) * scaled
    gain = tree(gain, near_n, 1)
    grad_gain = tree(gain, far_n, near_n)

    d_outs = gather_near(d_out, near_n)
    tokens = gather_near(inputs, near_n)
    d_pres, partial = [], {}
    for k in range(near_n):
        d_out_k = jnp.concatenate([d_outs[0][k], d_outs[1][k]], axis=0)
        d_out_k = [trade(d_out_k, "tp", t) for t in range(tp)]
        d_act = sum(dot(d_out_k[t], down[t], 1) for t in range(tp))
        d_pre = (d_act * 2.0 * jax.nn.relu(pre[k].astype(jnp.float32))).astype(jnp.bfloat16)
        d_pres.append([trade(d_pre, "tp", t) for t in range(tp)])
        partial[k] = sum(dot(d_pres[k][t], up[t], 1) for t in range(tp))
    grad_input = scatter_near(partial, near_n)

    all_pres = [
        jnp.concatenate([d_pres[k][t] for k in range(near_n)], axis=0) for t in range(tp)
    ]
    all_tokens = jnp.concatenate([side[k] for k in range(near_n) for side in tokens], axis=0)
    sums_up = [dot(x, all_tokens, 0) for x in all_pres]
    sums_up = jnp.concatenate(sums_up, axis=0).reshape(
        far_n, block, inputs.shape[1]
    )
    grad_up = 0.0
    for k in range(far_n):
        goal = far ^ k
        mine = pick(sums_up, (core ^ (goal // per)) * per + goal % per)
        if k:
            mine = trade(mine.astype(jnp.bfloat16), "fs", k * near_n).astype(jnp.float32)
        grad_up = grad_up + mine
    return (grad_input.astype(jnp.bfloat16), (grad_up * scaled).T, grad_gain)


def mm(a, b):
    return lax.dot_general(a, b, (((1,), (1,)), ((), ())), preferred_element_type=jnp.float32)


class Wire:
    def __init__(self, send, recv, other):
        self.send, self.recv, self.other = send, recv, other
        self.sent, self.came, self.pending = {}, {}, []

    def at(self, sems, names, key):
        index = names.setdefault(key, len(names))
        assert index < sems.shape[0], "semaphores"
        return sems.at[index]

    def put(self, refs, key, device, live=None, tag=None):
        out = self.at(self.send, self.sent, (key, tag))
        arrival = self.at(self.recv, self.came, key)

        def copy():
            source, target = refs()
            return pltpu.make_async_remote_copy(
                src_ref=source, dst_ref=target, send_sem=out, recv_sem=arrival,
                device_id=device, device_id_type=MESH,
            )

        when(live, lambda: copy().start())
        self.pending.append((copy, live))

    def got(self, ref, key):
        pltpu.make_async_remote_copy(
            src_ref=ref, dst_ref=ref, send_sem=self.send.at[0],
            recv_sem=self.at(self.recv, self.came, key),
            device_id=self.other, device_id_type=MESH,
        ).wait_recv()

    def drain(self):
        for copy, live in self.pending:
            when(live, lambda: copy().wait_send())
        self.pending = []


def when(live, body):
    if live is None:
        body()
    else:
        pl.when(live)(body)


def both(a, b):
    return a if b is None else b if a is None else jnp.logical_and(a, b)


def fused(nz, ny, inp, pre, nrm, gain, wu, wd, cot, gi_out, gu_out, gg_out,
          nrm_v, cot_v, gain_v, st, st2, d_out, inp_v, inp_t, pre_v, dn, up, dp,
          part, gi_own, gi_send, gi_got, chain, y_send, y_got, acc, gu_v,
          gacc, gx, gx2, gy, gy2, gz, loc, send, recv):
    nx, f32, bf16 = 2, jnp.float32, jnp.bfloat16
    rows, half = inp.shape
    nq, _, blk, cols = wd.shape
    ns = nz * ny
    width = 2 * half
    wide = nx * cols
    chunks = 4
    step = rows // chunks
    high = half // nq
    scaled = (rows * nz * ny * nx) ** (-0.5)

    me, core = lax.axis_index("fs"), lax.axis_index("tp")
    x, y, z = me % nx, (me // nx) % ny, me // (nx * ny)
    at_x = (me + 1 - 2 * x, core)
    at_y = (me + nx * (1 - 2 * y), core)
    at_up = (me + nx * ny, core)
    at_down = (me - nx * ny, core)
    at_core = (me, 1 - core)
    at_z = [(lax.rem(z + k, nz) * nx * ny + y * nx + x, core) for k in range(1, nz)]
    wire = Wire(send, recv, at_core)
    low_end, top_end = z > 0, z < nz - 1

    def place(zz, yy):
        return lax.rem(zz * ny + yy + core * nq, ns)

    local = {}

    def load(name, refs):
        index = len(local)
        local[name] = (lambda: pltpu.make_async_copy(*refs(), loc.at[index]))
        local[name]().start()

    def ready(name):
        local[name]().wait()

    load("nrm", lambda: (nrm, nrm_v))
    load("cot", lambda: (cot, cot_v))
    load("gain", lambda: (gain, gain_v))

    def own_dn(q, xx):
        start = place(z, y) * wide + xx * cols
        return dn.at[pl.ds(q * blk, blk), pl.ds(pl.multiple_of(start, cols), cols)]

    for q in range(nq):
        load(("dn", q), lambda q=q: (wd.at[q, x], own_dn(q, x)))
    for q in range(nq):
        load(("up", q), lambda q=q: (
            wu.at[pl.ds(q * high, high), :],
            up.at[pl.ds(q * high, high), pl.ds(pl.multiple_of(place(z, y) * blk, blk), blk)]))
    for q in range(nq):
        load(("pre", q), lambda q=q: (
            pre.at[:, pl.ds(pl.multiple_of((2 * q + x) * blk, blk), blk)], pre_v.at[0, q]))
    load("inp", lambda: (inp, inp_v.at[0]))

    barrier = pltpu.get_barrier_semaphore()
    peers = [at_core, at_x, at_y] + at_z
    for peer in peers:
        pl.semaphore_signal(barrier, inc=1, device_id=peer, device_id_type=MESH)
    pl.semaphore_wait(barrier, len(peers))

    for q in range(nq):
        wire.put(lambda q=q: (wd.at[q, 1 - x], own_dn(q, x)), ("swap", q), at_x)

    ready("nrm")
    ready("cot")
    ready("gain")
    gacc[...] = jnp.zeros_like(gacc)
    tall = 32

    def stats(i, carry):
        r = pl.ds(pl.multiple_of(i * tall, tall), tall)
        n = nrm_v[r, :].astype(f32)
        u = cot_v[r, :].astype(f32) * gain_v[...]
        squares = jnp.sum(n * n, axis=1, keepdims=True)
        cross = jnp.sum(u * n, axis=1, keepdims=True)
        lane = lax.broadcasted_iota(jnp.int32, (tall, st.shape[1]), 1)
        st[r, :] = jnp.where(lane == 0, squares, cross)
        return carry

    lax.fori_loop(0, rows // tall, stats, 0)
    wire.put(lambda: (st, st2), "stats", at_core)

    def piece(buf, tile, w, j, zz, yy):
        return buf.at[pl.ds(j * tile, tile), pl.ds(pl.multiple_of(place(zz, yy) * w, w), w)]

    gathers = {"dn": (dn, blk, wide), "up": (up, high, blk)}

    def spread(name, j, zz, tag, live, up_key, down_key, to_y=True, to_z=True):
        refs = lambda: (piece(*gathers[name], j, zz, y),) * 2
        if to_z and up_key is not None:
            wire.put(refs, (name, j, "u", up_key), at_up, both(live, top_end), tag)
        if to_z and down_key is not None:
            wire.put(refs, (name, j, "d", down_key), at_down, both(live, low_end), tag)
        if to_y:
            wire.put(refs, (name, j, "y", tag), at_y, live, "y")

    def own(name, j, **kw):
        spread(name, j, z, "own", None, 1, 1, **kw)

    def forward(name, j, k):
        below, above = z >= k, z + k < nz
        when(below, lambda: wire.got(piece(*gathers[name], j, z - k, y), (name, j, "u", k)))
        spread(name, j, z - k, ("u", k), below, k + 1 if k + 1 < nz else None, None)
        when(above, lambda: wire.got(piece(*gathers[name], j, z + k, y), (name, j, "d", k)))
        spread(name, j, z + k, ("d", k), above, None, k + 1 if k + 1 < nz else None)

    def arrived(name, j):
        wire.got(piece(*gathers[name], j, z, 1 - y), (name, j, "y", "own"))
        for k in range(1, nz):
            when(z >= k, lambda: wire.got(
                piece(*gathers[name], j, z - k, 1 - y), (name, j, "y", ("u", k))))
            when(z + k < nz, lambda: wire.got(
                piece(*gathers[name], j, z + k, 1 - y), (name, j, "y", ("d", k))))

    ready(("dn", 0))
    wire.got(own_dn(0, 1 - x), ("swap", 0))
    own("dn", 0)

    wire.got(st2, "stats")
    short = 16

    def norm(n_chunk):
        def rows_of(i, carry):
            r = pl.ds(pl.multiple_of(n_chunk * step + i * short, short), short)
            n = nrm_v[r, :].astype(f32)
            u = cot_v[r, :].astype(f32)
            both_sums = st[r, :] + st2[r, :]
            inv = lax.rsqrt(both_sums[:, 0:1] / width + norm_eps)
            cross = both_sums[:, 1:2] / width
            d = u * gain_v[...] * inv - n * (inv * inv * inv * cross)
            d_out[r, pl.ds(0, half)] = d.astype(bf16)
            g = u * n * inv
            gacc[...] += g[0:8] + g[8:16]
            return carry

        lax.fori_loop(0, step // short, rows_of, 0)

    def d_tile(t, n_chunk, h):
        return d_out.at[pl.ds(t * rows + n_chunk * step, step), pl.ds(h * half, half)]

    for n in range(chunks):
        norm(n)
        wire.put(lambda n=n: (d_tile(0, n, 0), d_tile(1, n, 0)), ("d_x", n), at_x)
        wire.put(lambda n=n: (d_tile(0, n, 0), d_tile(0, n, 1)), ("d_core", 0, n), at_core)

    for q in range(1, nq):
        ready(("dn", q))
        wire.got(own_dn(q, 1 - x), ("swap", q))
        own("dn", q)

    for q in range(nq):
        wire.put(lambda q=q: (
            pre.at[:, pl.ds(pl.multiple_of((2 * q + 1 - x) * blk, blk), blk)], pre_v.at[1, q]),
            ("pre", q), at_x)
    gx[...] = jnp.sum(gacc[...], axis=0, keepdims=True)
    wire.put(lambda: (gx, gx2), "gain_x", at_x)
    wire.put(lambda: (inp, inp_v.at[1]), "inp", at_x)

    def turn(t):
        def cols_of(i, carry):
            c = pl.ds(pl.multiple_of(i * blk, blk), blk)
            for k in range(half // blk):
                inp_t[pl.ds(k * blk, blk), pl.ds(pl.multiple_of(t * rows + i * blk, blk), blk)] = (
                    inp_v[t, c, pl.ds(k * blk, blk)].T)
            return carry

        lax.fori_loop(0, rows // blk, cols_of, 0)

    def act(t, q):
        def rows_of(i, carry):
            r = pl.ds(pl.multiple_of(t * rows + i * blk, blk), blk)
            got = mm(d_out[r, :], dn[pl.ds(q * blk, blk), :])
            p = pre_v[t, q, pl.ds(pl.multiple_of(i * blk, blk), blk), :].astype(f32)
            dp[r, pl.ds(q * blk, blk)] = (got * 2.0 * jnp.maximum(p, 0.0)).astype(bf16)
            return carry

        lax.fori_loop(0, rows // blk, rows_of, 0)
        tile = lambda s: dp.at[pl.ds(t * rows, rows), pl.ds((s * nq + q) * blk, blk)]
        wire.put(lambda: (tile(0), tile(1)), ("dp", t, q), at_core)

    for q in range(nq):
        for k in range(1, nz):
            forward("dn", q, k)
        if q < chunks:
            wire.got(d_tile(1, q, 0), ("d_x", q))
            wire.put(lambda q=q: (d_tile(1, q, 0), d_tile(1, q, 1)), ("d_core", 1, q), at_core)
        if q == 0:
            for n in range(chunks):
                wire.got(d_tile(0, n, 1), ("d_core", 0, n))
            ready("inp")
            turn(0)
        else:
            ready(("pre", q - 1))
            arrived("dn", q - 1)
            act(0, q - 1)
    for q in range(nq):
        ready(("up", q))
        own("up", q)
    ready(("pre", nq - 1))
    arrived("dn", nq - 1)
    act(0, nq - 1)

    wire.got(gx2, "gain_x")
    gy[...] = gx[...] + gx2[...]
    wire.put(lambda: (gy, gy2), "gain_y", at_y)

    for n in range(chunks):
        wire.got(d_tile(1, n, 1), ("d_core", 1, n))
    for q in range(nq):
        wire.got(pre_v.at[1, q], ("pre", q))
        act(1, q)
        for k in range(1, nz):
            forward("up", q, k)

    wire.got(gy2, "gain_y")
    gz[z] = gy[...] + gy2[...]
    for k, peer in enumerate(at_z):
        wire.put(lambda: (gz.at[z], gz.at[z]), ("gain_z", k), peer)

    for t in range(nx):
        for q in range(nq):
            wire.got(dp.at[pl.ds(t * rows, rows), pl.ds((nq + q) * blk, blk)], ("dp", t, q))

    def back(r):
        def rows_of(i, carry):
            k = pl.ds(pl.multiple_of(i * blk, blk), blk)
            w = up[pl.ds(r * high, high), :]
            far = mm(dp[pl.ds(pl.multiple_of(rows + i * blk, blk), blk), :], w)
            gi_send[r, k, :] = far.astype(bf16)
            return carry

        def rows_own(i, carry):
            k = pl.ds(pl.multiple_of(i * blk, blk), blk)
            w = up[pl.ds(r * high, high), :]
            gi_own[r, k, :] = mm(dp[k, :], w)
            return carry

        lax.fori_loop(0, rows // blk, rows_of, 0)
        wire.put(lambda: (gi_send.at[r], gi_got.at[r]), ("gi", r), at_x)
        lax.fori_loop(0, rows // blk, rows_own, 0)

    def grads(r):
        for j in range(ns):
            part[r, j] = lax.dot_general(
                inp_t[pl.ds(r * high, high), :], dp[:, pl.ds(j * blk, blk)],
                (((1,), (0,)), ((), ())), preferred_element_type=f32)

    def column(rel):
        return y if rel == 0 else 1 - y

    def link(kind, r, goal, rel):
        first, live, device = (
            (z == 0, z < goal, at_up) if kind == 0 else (z == nz - 1, z > goal, at_down))
        slot = chain.at[kind, r, goal, rel]
        key = ("sum", kind, r, goal, rel)

        def value():
            got = part[r, place(goal, column(rel))]
            return got + y_got[r, goal].astype(f32) if r >= split else got

        @pl.when(jnp.logical_and(live, first))
        def _():
            slot[...] = value().astype(bf16)

        @pl.when(jnp.logical_and(live, jnp.logical_not(first)))
        def _():
            wire.got(slot, key)
            slot[...] = (value() + slot[...].astype(f32)).astype(bf16)

        wire.put(lambda: (slot, slot), key, device, live)

    def links(r):
        for i in range(nz - 1):
            for rel in range(ny if r < split else 1):
                link(0, r, nz - 1 - i, rel)
                link(1, r, i, rel)

    def collect(r, rel):
        acc[...] = part[r, place(z, column(rel))]
        for kind, live in ((0, z > 0), (1, z < nz - 1)):
            @pl.when(live)
            def _():
                slot = chain.at[kind, r, z, rel]
                for goal in range(nz):
                    when(z == goal, lambda: wire.got(slot, ("sum", kind, r, goal, rel)))
                acc[...] += slot[...].astype(f32)

    def to_y(r, goal):
        y_send[r, goal] = part[r, place(goal, 1 - y)].astype(bf16)
        wire.put(lambda: (y_send.at[r, goal], y_got.at[r, goal]), ("y", r, goal), at_y)

    def finish(r):
        gu_v[pl.ds(r * high, high), :] = acc[...] * scaled
        tile = pl.ds(r * high, high)
        load(("gu", r), lambda: (gu_v.at[tile, :], gu_out.at[tile, :]))

    split = nq // 2
    arrived("up", 0)
    back(0)
    arrived("up", 1)
    back(1)
    wire.got(inp_v.at[1], "inp")
    turn(1)
    for r in range(split):
        grads(r)
        links(r)
    for r in range(split, nq):
        grads(r)
        for goal in range(nz):
            to_y(r, goal)
    for r in range(2, nq):
        arrived("up", r)
        back(r)
    for r in range(split):
        collect(r, 1)
        y_send[r, 0] = acc[...].astype(bf16)
        wire.put(lambda r=r: (y_send.at[r, 0], y_got.at[r, 0]), ("y", r, 0), at_y)
    for r in range(split, nq):
        for goal in range(nz):
            wire.got(y_got.at[r, goal], ("y", r, goal))
        links(r)
    for k in range(nz - 1):
        source = lax.rem(z + nz - 1 - k, nz)
        wire.got(gz.at[source], ("gain_z", k))
    total = gz[0]
    for k in range(1, nz):
        total = total + gz[k]
    gx2[...] = total * scaled
    load("gg", lambda: (gx2, gg_out))
    for r in range(nq):
        wire.got(gi_got.at[r], ("gi", r))
        inp_v[0, :, pl.ds(r * high, high)] = (gi_own[r] + gi_got[r].astype(f32)).astype(bf16)
    load("gi", lambda: (inp_v.at[0], gi_out))
    for r in range(split):
        collect(r, 0)
        wire.got(y_got.at[r, 0], ("y", r, 0))
        acc[...] += y_got[r, 0].astype(f32)
        finish(r)
    for r in range(split, nq):
        collect(r, 0)
        acc[...] += y_got[r, z].astype(f32)
        finish(r)
    wire.drain()
    for name in ["gg", "gi"] + [("gu", r) for r in range(nq)]:
        ready(name)


def kernel_step(fs, tp, inputs, hidden_pre, norm_input, out_gain, w_up, w_down, cotangent):
    nx = ny = 2
    nz = fs // (nx * ny)
    rows, half = inputs.shape
    blk, cols = w_up.shape[1], w_down.shape[1]
    nq = nz * ny // tp
    ns, high = nz * ny, half // nq
    hid = nq * blk
    f32, bf16 = jnp.float32, jnp.bfloat16
    v = pltpu.VMEM
    scratch = [
        v((rows, half), bf16), v((rows, half), bf16), v((1, half), f32),
        v((rows, 128), f32), v((rows, 128), f32),
        v((nx * rows, 2 * half), bf16),
        v((nx, rows, half), bf16), v((half, nx * rows), bf16),
        v((nx, nq, rows, blk), bf16),
        v((hid, 2 * half), bf16), v((half, ns * blk), bf16), v((nx * rows, ns * blk), bf16),
        v((nq, ns, high, blk), f32),
        v((nq, rows, high), f32), v((nq, rows, high), bf16), v((nq, rows, high), bf16),
        v((2, nq, nz, ny, high, blk), bf16),
        v((nq, nz, high, blk), bf16), v((nq, nz, high, blk), bf16),
        v((high, blk), f32), v((half, blk), f32),
        v((8, half), f32),
        v((1, half), f32), v((1, half), f32), v((1, half), f32), v((1, half), f32),
        v((nz, 1, half), f32),
        pltpu.SemaphoreType.DMA((3 + 3 * nq + 1 + 2 + nq,)),
        pltpu.SemaphoreType.DMA((SEMS,)), pltpu.SemaphoreType.DMA((SEMS,)),
    ]
    flops = 3 * 2 * nx * rows * 2 * half * hid
    grad_input, grad_up, grad_gain = pl.pallas_call(
        functools.partial(fused, nz, ny),
        out_shape=(
            jax.ShapeDtypeStruct((rows, half), bf16),
            jax.ShapeDtypeStruct((half, blk), f32),
            jax.ShapeDtypeStruct((1, half), f32),
        ),
        in_specs=[pl.BlockSpec(memory_space=pl.ANY)] * 7,
        out_specs=(pl.BlockSpec(memory_space=pl.ANY),) * 3,
        scratch_shapes=scratch,
        compiler_params=pltpu.CompilerParams(
            collective_id=0, has_side_effects=True, vmem_limit_bytes=67_000_000
        ),
        cost_estimate=pl.CostEstimate(flops=flops, bytes_accessed=1 << 24, transcendentals=0),
        name="layer_backward",
    )(
        inputs, hidden_pre, norm_input, out_gain.reshape(1, half), w_up,
        w_down.reshape(nq, nx, blk, cols), cotangent,
    )
    return grad_input, grad_up, grad_gain.reshape(half)


def in_kernel(*args):
    return kernel_step(lax.axis_size("fs"), lax.axis_size("tp"), *args)


def solution(mesh):
    placed = (
        P("fs", "tp"),
        P("fs", "tp"),
        P("fs", "tp"),
        P("tp"),
        P("tp", "fs"),
        P("tp", "fs"),
        P("fs", "tp"),
    )
    fs, tp = mesh.shape["fs"], mesh.shape["tp"]
    out_specs = (P("fs", "tp"), P("tp", "fs"), P("tp"))

    def solve(*args):
        up, down = args[4].shape, args[5].shape
        if tp == 2 and fs % 8 == 0 and up[1] // fs % 256 == 0 and down[1] // fs % 128 == 0:
            return jax.shard_map(
                in_kernel, mesh=mesh, in_specs=placed, out_specs=out_specs, check_vma=False
            )(*args)
        return permuted(*args)

    step = jax.shard_map(
        on_device,
        mesh=mesh,
        in_specs=placed,
        out_specs=(P("fs", "tp"), P("tp", "fs"), P("tp")),
        check_vma=False,
    )
    permuted = step
    return solve
```

profile of v0, /device:TPU:0, one launch (start us, length us, event | category | flops | bytes accessed | tf_op | source)
XLA Modules:
  0.0 185.5 jit_solution(8439510166733414833)
XLA Ops:
  0.6 180.9 %layer_backward.1 = (bf16[512,1024]{1,0:T(8,128)(2,1)}, f32[1024,256]{1,0:T(8,128)}, f32[1,1024]{1,0:T(1,128)}) custom-call(bf16[512,1024]{1,0:T(8,128)(2,1)} %inp.1, bf16[512,2048]{1,0:T(8,128)(2,1)} %pre.1, bf16[512,1024]{1,0:T(8,128)(2,1)} %nrm.1, f32[1,1024]{1,0:T(1,128)} %bitcast.5, bf16[1024,256]{1,0:T(8,128)(2,1)} %wu.1, ...), custom_call_target="tpu_custom_call" | custom-call | flops 12884901888 | bytes 16777216 | tf_op jit(solution)/shard_map/layer_backward/pallas_call | solution.py:604
  181.5 0.0 copy-start
  181.5 0.0 copy-start.1
  181.6 2.3 %copy.13 = bf16[512,1024]{1,0:T(8,128)(2,1)} copy(bf16[512,1024]{1,0:T(8,128)(2,1)} %get-tuple-element.12) | data formatting | bytes 2097152
  183.9 0.0 copy-done
  183.9 1.0 copy.14
  184.9 0.0 copy-done.1
  184.9 0.6 copy.15
Async XLA Ops:
  181.5 2.4 %copy-start = (f32[1024,256]{1,0:T(8,128)S(1)}, f32[1024,256]{1,0:T(8,128)}, u32[]{:S(2)}) copy-start(f32[1024,256]{1,0:T(8,128)} %get-tuple-element.13) | copy-start | bytes 3145732
  181.5 3.3 %copy-start.1 = (f32[1,1024]{1,0:T(1,128)S(1)}, f32[1,1024]{1,0:T(1,128)}, u32[]{:S(2)}) copy-start(f32[1,1024]{1,0:T(1,128)} %get-tuple-element.8) | copy-start | bytes 12292
where the time goes:
time: 186 us; the launch traced here: 185 us
  Pallas kernels  181 us (97%)
  local copies, waits for them, and re-layouts  3.92 us (2%)
    pallas_call x1, Pallas kernels, kernel_step(): pl.pallas_call(functools.partial(fused, nz, ny), out_shape=(jax.ShapeDtyp...  181 us
    unnamed x7, local copies, waits for them, and re-layouts  3.92 us

commit v1 on v0

--- a/solution.py
+++ b/solution.py
@@ -10,7 +10,7 @@
 
 norm_eps = 1e-06
 MESH = pl.DeviceIdType.MESH
-SEMS = 256
+SEMS = 320
 
 
 def trade(x, axis, mask):
@@ -223,7 +223,7 @@
 
 def fused(nz, ny, inp, pre, nrm, gain, wu, wd, cot, gi_out, gu_out, gg_out,
           nrm_v, cot_v, gain_v, st, st2, d_out, inp_v, inp_t, pre_v, dn, up, dp,
-          part, gi_own, gi_send, gi_got, chain, y_send, y_got, acc, gu_v,
+          part, gi_own, gi_send, gi_got, chain, y_send, y_got, acc,
           gacc, gx, gx2, gy, gy2, gz, loc, send, recv):
     nx, f32, bf16 = 2, jnp.float32, jnp.bfloat16
     rows, half = inp.shape
@@ -243,9 +243,12 @@
     at_up = (me + nx * ny, core)
     at_down = (me - nx * ny, core)
     at_core = (me, 1 - core)
-    at_z = [(lax.rem(z + k, nz) * nx * ny + y * nx + x, core) for k in range(1, nz)]
+    at_up2 = (me + 2 * nx * ny, core)
+    at_down2 = (me - 2 * nx * ny, core)
     wire = Wire(send, recv, at_core)
     low_end, top_end = z > 0, z < nz - 1
+    low2, top2 = z > 1, z < nz - 2
+    reach = 1
 
     def place(zz, yy):
         return lax.rem(zz * ny + yy + core * nq, ns)
@@ -280,10 +283,16 @@
     load("inp", lambda: (inp, inp_v.at[0]))
 
     barrier = pltpu.get_barrier_semaphore()
-    peers = [at_core, at_x, at_y] + at_z
-    for peer in peers:
-        pl.semaphore_signal(barrier, inc=1, device_id=peer, device_id_type=MESH)
-    pl.semaphore_wait(barrier, len(peers))
+    peers = (
+        (at_core, None), (at_x, None), (at_y, None), (at_up, top_end), (at_down, low_end),
+    ) + (((at_up2, top2), (at_down2, low2)) if reach > 1 else ())
+    for peer, live in peers:
+        when(live, lambda: pl.semaphore_signal(
+            barrier, inc=1, device_id=peer, device_id_type=MESH))
+    count = 3
+    for _, live in peers[3:]:
+        count = count + live.astype(jnp.int32)
+    pl.semaphore_wait(barrier, count)
 
     for q in range(nq):
         wire.put(lambda q=q: (wd.at[q, 1 - x], own_dn(q, x)), ("swap", q), at_x)
@@ -307,41 +316,77 @@
     lax.fori_loop(0, rows // tall, stats, 0)
     wire.put(lambda: (st, st2), "stats", at_core)
 
-    def piece(buf, tile, w, j, zz, yy):
-        return buf.at[pl.ds(j * tile, tile), pl.ds(pl.multiple_of(place(zz, yy) * w, w), w)]
+    def piece(name, j, zz, yy, part_of=0):
+        buf, tile, w = gathers[name]
+        first = (0, 0, tile // 2)[part_of]
+        count = (tile, tile // 2, tile // 2)[part_of]
+        return buf.at[pl.ds(j * tile + first, count),
+                      pl.ds(pl.multiple_of(place(zz, yy) * w, w), w)]
 
     gathers = {"dn": (dn, blk, wide), "up": (up, high, blk)}
-
-    def spread(name, j, zz, tag, live, up_key, down_key, to_y=True, to_z=True):
-        refs = lambda: (piece(*gathers[name], j, zz, y),) * 2
-        if to_z and up_key is not None:
-            wire.put(refs, (name, j, "u", up_key), at_up, both(live, top_end), tag)
-        if to_z and down_key is not None:
-            wire.put(refs, (name, j, "d", down_key), at_down, both(live, low_end), tag)
-        if to_y:
-            wire.put(refs, (name, j, "y", tag), at_y, live, "y")
-
-    def own(name, j, **kw):
-        spread(name, j, z, "own", None, 1, 1, **kw)
+    odd = z % 2 == 1
+    even = jnp.logical_not(odd)
+
+    def over_y(name, j, zz, tag, live, halved=None):
+        refs = lambda: (piece(name, j, zz, y),) * 2
+        half_refs = lambda: (piece(name, j, zz, y, 1),) * 2
+        key = (name, j, "y", tag)
+        if halved is None:
+            wire.put(refs, key, at_y, live, "y")
+        else:
+            wire.put(refs, key, at_y, both(live, jnp.logical_not(halved)), "y")
+            wire.put(half_refs, key, at_y, both(live, halved), "y")
+
+    def own(name, j):
+        refs = lambda: (piece(name, j, z, y),) * 2
+        wire.put(refs, (name, j, "u", 1), at_up, top_end)
+        wire.put(refs, (name, j, "d", 1), at_down, low_end)
+        over_y(name, j, z, "own", None)
+        if reach > 1:
+            wire.put(refs, (name, j, "u", 2), at_up2, top2)
+            wire.put(refs, (name, j, "d", 2), at_down2, low2)
 
     def forward(name, j, k):
-        below, above = z >= k, z + k < nz
-        when(below, lambda: wire.got(piece(*gathers[name], j, z - k, y), (name, j, "u", k)))
-        spread(name, j, z - k, ("u", k), below, k + 1 if k + 1 < nz else None, None)
-        when(above, lambda: wire.got(piece(*gathers[name], j, z + k, y), (name, j, "d", k)))
-        spread(name, j, z + k, ("d", k), above, None, k + 1 if k + 1 < nz else None)
+        for way, zz, live, device, ahead, halved in (
+            ("u", z - k, z >= k, at_up, top_end, odd),
+            ("d", z + k, z + k < nz, at_down, low_end, even),
+        ):
+            when(live, lambda: wire.got(piece(name, j, zz, y), (name, j, way, k)))
+            if reach <= k < nz - 1:
+                wire.put(lambda zz=zz: (piece(name, j, zz, y),) * 2, (name, j, way, k + 1),
+                         device, both(live, ahead))
+            over_y(name, j, zz, (way, k), live, halved if k == 1 else None)
+
+    def side(name, j):
+        wire.got(piece(name, j, z, 1 - y), (name, j, "y", "own"))
+        refs = lambda: (piece(name, j, z, 1 - y, 2),) * 2
+        wire.put(refs, (name, j, "side"), at_up, even)
+        wire.put(refs, (name, j, "side"), at_down, odd)
 
     def arrived(name, j):
-        wire.got(piece(*gathers[name], j, z, 1 - y), (name, j, "y", "own"))
         for k in range(1, nz):
-            when(z >= k, lambda: wire.got(
-                piece(*gathers[name], j, z - k, 1 - y), (name, j, "y", ("u", k))))
-            when(z + k < nz, lambda: wire.got(
-                piece(*gathers[name], j, z + k, 1 - y), (name, j, "y", ("d", k))))
-
-    ready(("dn", 0))
-    wire.got(own_dn(0, 1 - x), ("swap", 0))
-    own("dn", 0)
+            for tag, zz, live, halved in (
+                ("u", z - k, z >= k, odd), ("d", z + k, z + k < nz, even)
+            ):
+                key = (name, j, "y", (tag, k))
+                if k == 1:
+                    when(jnp.logical_and(live, halved), lambda: wire.got(
+                        piece(name, j, zz, 1 - y, 1), key))
+                    live = jnp.logical_and(live, jnp.logical_not(halved))
+                when(live, lambda: wire.got(piece(name, j, zz, 1 - y), key))
+        wire.got(piece(name, j, z + 1 - 2 * (z % 2), 1 - y, 2), (name, j, "side"))
+
+    order = [("up", 0)] + [("dn", q) for q in range(nq)] + [("up", q) for q in range(1, nq)]
+
+    def next_piece(p):
+        if p < len(order):
+            name, j = order[p]
+            ready((name, j))
+            if name == "dn":
+                wire.got(own_dn(j, 1 - x), ("swap", j))
+            own(name, j)
+
+    next_piece(0)
 
     wire.got(st2, "stats")
     short = 16
@@ -370,18 +415,13 @@
         wire.put(lambda n=n: (d_tile(0, n, 0), d_tile(1, n, 0)), ("d_x", n), at_x)
         wire.put(lambda n=n: (d_tile(0, n, 0), d_tile(0, n, 1)), ("d_core", 0, n), at_core)
 
-    for q in range(1, nq):
-        ready(("dn", q))
-        wire.got(own_dn(q, 1 - x), ("swap", q))
-        own("dn", q)
-
+    gx[...] = jnp.sum(gacc[...], axis=0, keepdims=True)
+    wire.put(lambda: (gx, gx2), "gain_x", at_x)
+    wire.put(lambda: (inp, inp_v.at[1]), "inp", at_x)
     for q in range(nq):
         wire.put(lambda q=q: (
             pre.at[:, pl.ds(pl.multiple_of((2 * q + 1 - x) * blk, blk), blk)], pre_v.at[1, q]),
             ("pre", q), at_x)
-    gx[...] = jnp.sum(gacc[...], axis=0, keepdims=True)
-    wire.put(lambda: (gx, gx2), "gain_x", at_x)
-    wire.put(lambda: (inp, inp_v.at[1]), "inp", at_x)
 
     def turn(t):
         def cols_of(i, carry):
@@ -405,48 +445,30 @@
         tile = lambda s: dp.at[pl.ds(t * rows, rows), pl.ds((s * nq + q) * blk, blk)]
         wire.put(lambda: (tile(0), tile(1)), ("dp", t, q), at_core)
 
-    for q in range(nq):
-        for k in range(1, nz):
-            forward("dn", q, k)
-        if q < chunks:
-            wire.got(d_tile(1, q, 0), ("d_x", q))
-            wire.put(lambda q=q: (d_tile(1, q, 0), d_tile(1, q, 1)), ("d_core", 1, q), at_core)
+    def relay(p, k):
+        forward(*order[p], k)
+        if k == 1:
+            side(*order[p])
+            next_piece(p + 3)
+
+    def d_back(n):
+        wire.got(d_tile(1, n, 0), ("d_x", n))
+        wire.put(lambda: (d_tile(1, n, 0), d_tile(1, n, 1)), ("d_core", 1, n), at_core)
+
+    def act_own(q):
         if q == 0:
             for n in range(chunks):
                 wire.got(d_tile(0, n, 1), ("d_core", 0, n))
-            ready("inp")
-            turn(0)
-        else:
-            ready(("pre", q - 1))
-            arrived("dn", q - 1)
-            act(0, q - 1)
-    for q in range(nq):
-        ready(("up", q))
-        own("up", q)
-    ready(("pre", nq - 1))
-    arrived("dn", nq - 1)
-    act(0, nq - 1)
-
-    wire.got(gx2, "gain_x")
-    gy[...] = gx[...] + gx2[...]
-    wire.put(lambda: (gy, gy2), "gain_y", at_y)
-
-    for n in range(chunks):
-        wire.got(d_tile(1, n, 1), ("d_core", 1, n))
-    for q in range(nq):
+        ready(("pre", q))
+        arrived("dn", q)
+        act(0, q)
+
+    def act_far(q):
+        if q == 0:
+            for n in range(chunks):
+                wire.got(d_tile(1, n, 1), ("d_core", 1, n))
         wire.got(pre_v.at[1, q], ("pre", q))
         act(1, q)
-        for k in range(1, nz):
-            forward("up", q, k)
-
-    wire.got(gy2, "gain_y")
-    gz[z] = gy[...] + gy2[...]
-    for k, peer in enumerate(at_z):
-        wire.put(lambda: (gz.at[z], gz.at[z]), ("gain_z", k), peer)
-
-    for t in range(nx):
-        for q in range(nq):
-            wire.got(dp.at[pl.ds(t * rows, rows), pl.ds((nq + q) * blk, blk)], ("dp", t, q))
 
     def back(r):
         def rows_of(i, carry):
@@ -466,110 +488,241 @@
         wire.put(lambda: (gi_send.at[r], gi_got.at[r]), ("gi", r), at_x)
         lax.fori_loop(0, rows // blk, rows_own, 0)
 
-    def grads(r):
-        for j in range(ns):
-            part[r, j] = lax.dot_general(
-                inp_t[pl.ds(r * high, high), :], dp[:, pl.ds(j * blk, blk)],
-                (((1,), (0,)), ((), ())), preferred_element_type=f32)
-
-    def column(rel):
-        return y if rel == 0 else 1 - y
-
-    def link(kind, r, goal, rel):
-        first, live, device = (
-            (z == 0, z < goal, at_up) if kind == 0 else (z == nz - 1, z > goal, at_down))
-        slot = chain.at[kind, r, goal, rel]
-        key = ("sum", kind, r, goal, rel)
-
-        def value():
-            got = part[r, place(goal, column(rel))]
-            return got + y_got[r, goal].astype(f32) if r >= split else got
-
-        @pl.when(jnp.logical_and(live, first))
-        def _():
-            slot[...] = value().astype(bf16)
-
-        @pl.when(jnp.logical_and(live, jnp.logical_not(first)))
-        def _():
-            wire.got(slot, key)
-            slot[...] = (value() + slot[...].astype(f32)).astype(bf16)
-
-        wire.put(lambda: (slot, slot), key, device, live)
-
-    def links(r):
-        for i in range(nz - 1):
-            for rel in range(ny if r < split else 1):
-                link(0, r, nz - 1 - i, rel)
-                link(1, r, i, rel)
-
-    def collect(r, rel):
-        acc[...] = part[r, place(z, column(rel))]
-        for kind, live in ((0, z > 0), (1, z < nz - 1)):
+    def grads(q):
+        for t in range(nx):
+            wire.got(dp.at[pl.ds(t * rows, rows), pl.ds((nq + q) * blk, blk)], ("dp", t, q))
+        for j in (q, nq + q):
+            for r in range(nq):
+                part[r, j] = lax.dot_general(
+                    inp_t[pl.ds(r * high, high), :], dp[:, pl.ds(j * blk, blk)],
+                    (((1,), (0,)), ((), ())), preferred_element_type=f32)
+
+    def goals(q):
+        return [divmod(b, ny) for b in (q, nq + q)]
+
+    def first_y(r):
+        return r >= split
+
+    def to_y(q, r):
+        for goal, column in goals(q):
+            live = y != column
+
             @pl.when(live)
             def _():
-                slot = chain.at[kind, r, z, rel]
-                for goal in range(nz):
-                    when(z == goal, lambda: wire.got(slot, ("sum", kind, r, goal, rel)))
-                acc[...] += slot[...].astype(f32)
-
-    def to_y(r, goal):
-        y_send[r, goal] = part[r, place(goal, 1 - y)].astype(bf16)
-        wire.put(lambda: (y_send.at[r, goal], y_got.at[r, goal]), ("y", r, goal), at_y)
-
-    def finish(r):
-        gu_v[pl.ds(r * high, high), :] = acc[...] * scaled
-        tile = pl.ds(r * high, high)
-        load(("gu", r), lambda: (gu_v.at[tile, :], gu_out.at[tile, :]))
+                y_send[r, goal] = part[r, place(goal, column)].astype(bf16)
+
+            wire.put(lambda goal=goal: (y_send.at[r, goal], y_got.at[r, goal]),
+                     ("y", r, goal), at_y, live)
+
+    def link(q, r, level):
+        for goal, column in goals(q):
+            for kind in range(2):
+                at = level if kind == 0 else nz - 1 - level
+                if at >= goal if kind == 0 else at <= goal:
+                    continue
+                slot = chain.at[kind, r, goal, column]
+                key = ("sum", kind, r, goal, column)
+                live = z == at
+                if first_y(r):
+                    live = jnp.logical_and(live, y == column)
+
+                @pl.when(live)
+                def _():
+                    value = part[r, place(goal, column)]
+                    if first_y(r):
+                        wire.got(y_got.at[r, goal], ("y", r, goal))
+                        value = value + y_got[r, goal].astype(f32)
+                    if level > 0:
+                        wire.got(slot, key)
+                        value = value + slot[...].astype(f32)
+                    slot[...] = value.astype(bf16)
+
+                wire.put(lambda slot=slot: (slot, slot), key,
+                         at_up if kind == 0 else at_down, live)
+
+    def settle(q, r):
+        for goal, column in goals(q):
+            live = z == goal
+            if first_y(r):
+                live = jnp.logical_and(live, y == column)
+
+            @pl.when(live)
+            def _():
+                value = part[r, place(goal, column)]
+                if first_y(r):
+                    wire.got(y_got.at[r, goal], ("y", r, goal))
+                    value = value + y_got[r, goal].astype(f32)
+                for kind in range(2):
+                    if goal != (0, nz - 1)[kind]:
+                        slot = chain.at[kind, r, goal, column]
+                        wire.got(slot, ("sum", kind, r, goal, column))
+                        value = value + slot[...].astype(f32)
+                if first_y(r):
+                    gu_out[pl.ds(r * high, high), :] = value * scaled
+                else:
+                    acc[r] = value
+
+            if not first_y(r):
+                away = jnp.logical_and(live, y != column)
+
+                @pl.when(away)
+                def _():
+                    y_send[r, 0] = acc[r].astype(bf16)
+
+                @pl.when(jnp.logical_and(live, y == column))
+                def _():
+                    gu_out[pl.ds(r * high, high), :] = acc[r]
+
+                wire.put(lambda: (y_send.at[r, 0], y_got.at[r, 0]), ("y", r), at_y, away)
 
     split = nq // 2
+    first = list(range(split))
+    later = list(range(split, nq))
+
+    def step_of(rows_set, q, level):
+        for r in rows_set:
+            if level < nz - 1:
+                link(q, r, level)
+            else:
+                settle(q, r)
+
+    def z_step(q, level):
+        step_of(first, q, level)
+
+    def y_step(q, level):
+        step_of(later, q, level)
+
+    def gain_over_y():
+        wire.got(gx2, "gain_x")
+        gy[...] = gx[...] + gx2[...]
+        wire.put(lambda: (gy, gy2), "gain_y", at_y)
+
+    def gain_over_z():
+        wire.got(gy2, "gain_y")
+        gz[z] = gy[...] + gy2[...]
+        wire.put(lambda: (gz.at[z], gz.at[z]), ("gain", "u", 1), at_up, top_end)
+        wire.put(lambda: (gz.at[z], gz.at[z]), ("gain", "d", 1), at_down, low_end)
+
+    def over_rows(q):
+        for r in later:
+            to_y(q, r)
+
+    def gain_relay(k):
+        for key, slot, live, device, ahead in (
+            ("u", z - k, z >= k, at_up, top_end), ("d", z + k, z + k < nz, at_down, low_end)
+        ):
+            when(live, lambda: wire.got(gz.at[slot], ("gain", key, k)))
+            if k + 1 < nz:
+                wire.put(lambda slot=slot: (gz.at[slot], gz.at[slot]), ("gain", key, k + 1),
+                         device, both(live, ahead))
+
+    for p in range(1, 3):
+        next_piece(p)
+    relay(0, 1)
+    relay(1, 1)
+    relay(0, 2)
+    relay(2, 1)
+    d_back(0)
+    relay(1, 2)
+    relay(2, 2)
+    relay(3, 1)
+    relay(0, 3)
+    relay(1, 3)
+    relay(2, 3)
+    d_back(1)
+    ready("inp")
+    turn(0)
+    d_back(2)
+    d_back(3)
+    gain_over_y()
+    relay(4, 1)
+    act_own(0)
+    relay(3, 2)
+    relay(4, 2)
+    relay(5, 1)
+    wire.got(inp_v.at[1], "inp")
+    turn(1)
+    act_own(1)
+    relay(6, 1)
+    gain_over_z()
+    act_far(0)
+    grads(0)
+    relay(3, 3)
+    z_step(0, 0)
+    act_far(1)
+    relay(4, 3)
+    grads(1)
+    z_step(1, 0)
+    act_own(2)
+    act_far(2)
+    relay(5, 2)
+    relay(6, 2)
+    relay(7, 1)
+    grads(2)
+    gain_relay(1)
+    z_step(2, 0)
+    relay(5, 3)
+    z_step(0, 1)
+    relay(6, 3)
+    act_own(3)
+    act_far(3)
+    grads(3)
+    over_rows(3)
+    over_rows(2)
+    over_rows(0)
+    z_step(0, 2)
+    z_step(3, 0)
+    arrived("up", 1)
+    back(1)
+    over_rows(1)
+    relay(7, 2)
+    gain_relay(2)
+    z_step(1, 1)
+    relay(7, 3)
+    y_step(3, 0)
+    y_step(2, 0)
+    arrived("up", 2)
+    back(2)
+    y_step(0, 0)
+    z_step(2, 1)
+    y_step(1, 0)
+    z_step(2, 2)
+    z_step(3, 1)
+    z_step(1, 2)
+    z_step(1, 3)
+    z_step(3, 2)
+    z_step(3, 3)
+    y_step(3, 1)
+    gain_relay(3)
+    y_step(2, 1)
     arrived("up", 0)
     back(0)
-    arrived("up", 1)
-    back(1)
-    wire.got(inp_v.at[1], "inp")
-    turn(1)
-    for r in range(split):
-        grads(r)
-        links(r)
-    for r in range(split, nq):
-        grads(r)
-        for goal in range(nz):
-            to_y(r, goal)
-    for r in range(2, nq):
-        arrived("up", r)
-        back(r)
-    for r in range(split):
-        collect(r, 1)
-        y_send[r, 0] = acc[...].astype(bf16)
-        wire.put(lambda r=r: (y_send.at[r, 0], y_got.at[r, 0]), ("y", r, 0), at_y)
-    for r in range(split, nq):
-        for goal in range(nz):
-            wire.got(y_got.at[r, goal], ("y", r, goal))
-        links(r)
-    for k in range(nz - 1):
-        source = lax.rem(z + nz - 1 - k, nz)
-        wire.got(gz.at[source], ("gain_z", k))
+    arrived("up", 3)
+    back(3)
+    z_step(2, 3)
+    y_step(1, 1)
+    y_step(0, 1)
+    y_step(3, 2)
+    y_step(0, 2)
+    z_step(0, 3)
+    y_step(1, 2)
+    y_step(2, 2)
+    y_step(2, 3)
+    y_step(3, 3)
+    y_step(0, 3)
+    y_step(1, 3)
     total = gz[0]
     for k in range(1, nz):
         total = total + gz[k]
-    gx2[...] = total * scaled
-    load("gg", lambda: (gx2, gg_out))
+    gg_out[...] = total * scaled
     for r in range(nq):
         wire.got(gi_got.at[r], ("gi", r))
-        inp_v[0, :, pl.ds(r * high, high)] = (gi_own[r] + gi_got[r].astype(f32)).astype(bf16)
-    load("gi", lambda: (inp_v.at[0], gi_out))
-    for r in range(split):
-        collect(r, 0)
-        wire.got(y_got.at[r, 0], ("y", r, 0))
-        acc[...] += y_got[r, 0].astype(f32)
-        finish(r)
-    for r in range(split, nq):
-        collect(r, 0)
-        acc[...] += y_got[r, z].astype(f32)
-        finish(r)
+        gi_out[:, pl.ds(r * high, high)] = (gi_own[r] + gi_got[r].astype(f32)).astype(bf16)
+    for r in first:
+        wire.got(y_got.at[r, 0], ("y", r))
+        tile = pl.ds(r * high, high)
+        gu_out[tile, :] = (gu_out[tile, :] + y_got[r, 0].astype(f32)) * scaled
     wire.drain()
-    for name in ["gg", "gi"] + [("gu", r) for r in range(nq)]:
-        ready(name)
 
 
 def kernel_step(fs, tp, inputs, hidden_pre, norm_input, out_gain, w_up, w_down, cotangent):
@@ -593,26 +746,23 @@
         v((nq, rows, high), f32), v((nq, rows, high), bf16), v((nq, rows, high), bf16),
         v((2, nq, nz, ny, high, blk), bf16),
         v((nq, nz, high, blk), bf16), v((nq, nz, high, blk), bf16),
-        v((high, blk), f32), v((half, blk), f32),
+        v((nq // 2, high, blk), f32),
         v((8, half), f32),
         v((1, half), f32), v((1, half), f32), v((1, half), f32), v((1, half), f32),
         v((nz, 1, half), f32),
-        pltpu.SemaphoreType.DMA((3 + 3 * nq + 1 + 2 + nq,)),
+        pltpu.SemaphoreType.DMA((3 + 3 * nq + 1,)),
         pltpu.SemaphoreType.DMA((SEMS,)), pltpu.SemaphoreType.DMA((SEMS,)),
     ]
     flops = 3 * 2 * nx * rows * 2 * half * hid
-    grad_input, grad_up, grad_gain = pl.pallas_call(
+    shapes = ((rows, half), bf16), ((half, blk), f32), ((1, half), f32)
+    results = pl.pallas_call(
         functools.partial(fused, nz, ny),
-        out_shape=(
-            jax.ShapeDtypeStruct((rows, half), bf16),
-            jax.ShapeDtypeStruct((half, blk), f32),
-            jax.ShapeDtypeStruct((1, half), f32),
-        ),
+        out_shape=tuple(v(*shape) for shape in shapes),
         in_specs=[pl.BlockSpec(memory_space=pl.ANY)] * 7,
-        out_specs=(pl.BlockSpec(memory_space=pl.ANY),) * 3,
+        out_specs=(pl.BlockSpec(memory_space=pltpu.VMEM),) * 3,
         scratch_shapes=scratch,
         compiler_params=pltpu.CompilerParams(
-            collective_id=0, has_side_effects=True, vmem_limit_bytes=67_000_000
+            collective_id=0, has_side_effects=True, vmem_limit_bytes=60 << 20
         ),
         cost_estimate=pl.CostEstimate(flops=flops, bytes_accessed=1 << 24, transcendentals=0),
         name="layer_backward",
@@ -620,6 +770,7 @@
         inputs, hidden_pre, norm_input, out_gain.reshape(1, half), w_up,
         w_down.reshape(nq, nx, blk, cols), cotangent,
     )
+    grad_input, grad_up, grad_gain = results
     return grad_input, grad_up, grad_gain.reshape(half)
 
 

time: 186 us -> 137 us (0.74)
  Pallas kernels: 181 us -> 134 us
    pallas_call x1, Pallas kernels: 181 us -> 134 us  [kernel_step(): pl.pallas_call(functools.partial(fused, nz, ny), out_shape=tuple((v(*shap...]
    unnamed x7 -> x3, local copies, waits for them, and re-layouts: 3.92 us -> 2.54 us
where the time goes in v1:
time: 137 us
  Pallas kernels  134 us (98%)
  local copies, waits for them, and re-layouts  2.54 us (2%)
    pallas_call x1, Pallas kernels, kernel_step(): pl.pallas_call(functools.partial(fused, nz, ny), out_shape=tuple((v(*shap...  134 us

profile of v1, /device:TPU:0, one launch (start us, length us, event | category | flops | bytes accessed | tf_op | source)
XLA Modules:
  0.0 137.4 jit_solution(8673006122249516699)
XLA Ops:
  0.6 134.2 %layer_backward.1 = (bf16[512,1024]{1,0:T(8,128)(2,1)S(1)}, f32[1024,256]{1,0:T(8,128)S(1)}, f32[1,1024]{1,0:T(1,128)S(1)}) custom-call(bf16[512,1024]{1,0:T(8,128)(2,1)} %inp.1, bf16[512,2048]{1,0:T(8,128)(2,1)} %pre.1, bf16[512,1024]{1,0:T(8,128)(2,1)} %nrm.1, f32[1,1024]{1,0:T(1,128)} %bitcast.5, bf16[1024,256]{1,0:T(8,128)(2,1)} %wu.1, ...), custom_call_target="tpu_custom_call" | custom-call | flops 12884901888 | bytes 16777216 | tf_op jit(solution)/shard_map/layer_backward/pallas_call | solution.py:758
  134.8 1.0 copy.13
  135.8 0.6 copy.15
  136.4 1.0 copy.14

commit v2 on v1

--- a/solution.py
+++ b/solution.py
@@ -10,7 +10,12 @@
 
 norm_eps = 1e-06
 MESH = pl.DeviceIdType.MESH
-SEMS = 320
+SENDS = 170
+RECVS = 160
+PLAN_STEPS = 4
+FULL_SIDE = ()
+Y_FIRST = ((0, 3), (1, 3), (2, 2), (2, 3), (3, 0), (3, 3))
+X_ORDER = (("pre", 0), ("inp", 0), ("inp", 2), ("pre", 2), ("inp", 1), ("pre", 1), ("pre", 3), ("inp", 3))
 
 
 def trade(x, axis, mask):
@@ -174,18 +179,36 @@
 
 
 class Wire:
-    def __init__(self, send, recv, other):
-        self.send, self.recv, self.other = send, recv, other
+    def __init__(self, send, recv, other, nz):
+        self.send, self.recv, self.other, self.nz = send, recv, other, nz
         self.sent, self.came, self.pending = {}, {}, []
+
+    def arrives(self, key):
+        *head, way, k = key if isinstance(key, tuple) else (key, None, None)
+        if key[0] == "sum":
+            kind, r, goal, column = key[1:]
+            return "sum", r, goal + 1 - kind, column
+        if way == "d":
+            return *head, "u", self.nz - k
+        if way == "y" and k[0] == "d":
+            return *head, "y", ("u", self.nz - k[1])
+        return key
+
+    def departs(self, key):
+        if key[0] == "sum":
+            return "sum", *key[2:]
+        if isinstance(key, tuple) and key[-2] == "d":
+            return key if key[-1] < self.nz - 1 else (*key[:-2], "u", key[-1])
+        return self.arrives(key)
 
     def at(self, sems, names, key):
         index = names.setdefault(key, len(names))
         assert index < sems.shape[0], "semaphores"
         return sems.at[index]
 
-    def put(self, refs, key, device, live=None, tag=None):
-        out = self.at(self.send, self.sent, (key, tag))
-        arrival = self.at(self.recv, self.came, key)
+    def put(self, refs, key, device, live=None):
+        out = self.at(self.send, self.sent, self.departs(key))
+        arrival = self.at(self.recv, self.came, self.arrives(key))
 
         def copy():
             source, target = refs()
@@ -200,7 +223,7 @@
     def got(self, ref, key):
         pltpu.make_async_remote_copy(
             src_ref=ref, dst_ref=ref, send_sem=self.send.at[0],
-            recv_sem=self.at(self.recv, self.came, key),
+            recv_sem=self.at(self.recv, self.came, self.arrives(key)),
             device_id=self.other, device_id_type=MESH,
         ).wait_recv()
 
@@ -223,8 +246,8 @@
 
 def fused(nz, ny, inp, pre, nrm, gain, wu, wd, cot, gi_out, gu_out, gg_out,
           nrm_v, cot_v, gain_v, st, st2, d_out, inp_v, inp_t, pre_v, dn, up, dp,
-          part, gi_own, gi_send, gi_got, chain, y_send, y_got, acc,
-          gacc, gx, gx2, gy, gy2, gz, loc, send, recv):
+          part, gi_own, gi_send, gi_got, chain, y_send, y_got,
+          tot_send, tot_got, acc, gacc, gx, gx2, gy, gy2, gz, loc, send, recv):
     nx, f32, bf16 = 2, jnp.float32, jnp.bfloat16
     rows, half = inp.shape
     nq, _, blk, cols = wd.shape
@@ -243,12 +266,8 @@
     at_up = (me + nx * ny, core)
     at_down = (me - nx * ny, core)
     at_core = (me, 1 - core)
-    at_up2 = (me + 2 * nx * ny, core)
-    at_down2 = (me - 2 * nx * ny, core)
-    wire = Wire(send, recv, at_core)
+    wire = Wire(send, recv, at_core, nz)
     low_end, top_end = z > 0, z < nz - 1
-    low2, top2 = z > 1, z < nz - 2
-    reach = 1
 
     def place(zz, yy):
         return lax.rem(zz * ny + yy + core * nq, ns)
@@ -285,17 +304,13 @@
     barrier = pltpu.get_barrier_semaphore()
     peers = (
         (at_core, None), (at_x, None), (at_y, None), (at_up, top_end), (at_down, low_end),
-    ) + (((at_up2, top2), (at_down2, low2)) if reach > 1 else ())
+    )
     for peer, live in peers:
         when(live, lambda: pl.semaphore_signal(
             barrier, inc=1, device_id=peer, device_id_type=MESH))
     count = 3
     for _, live in peers[3:]:
         count = count + live.astype(jnp.int32)
-    pl.semaphore_wait(barrier, count)
-
-    for q in range(nq):
-        wire.put(lambda q=q: (wd.at[q, 1 - x], own_dn(q, x)), ("swap", q), at_x)
 
     ready("nrm")
     ready("cot")
@@ -314,7 +329,13 @@
         return carry
 
     lax.fori_loop(0, rows // tall, stats, 0)
+
+    pl.semaphore_wait(barrier, count)
+
     wire.put(lambda: (st, st2), "stats", at_core)
+    for q in range(nq):
+        wire.put(lambda q=q: (wd.at[q, 1 - x], own_dn(q, x)), ("swap", q), at_x)
+
 
     def piece(name, j, zz, yy, part_of=0):
         buf, tile, w = gathers[name]
@@ -332,19 +353,17 @@
         half_refs = lambda: (piece(name, j, zz, y, 1),) * 2
         key = (name, j, "y", tag)
         if halved is None:
-            wire.put(refs, key, at_y, live, "y")
+            wire.put(refs, key, at_y, live)
         else:
-            wire.put(refs, key, at_y, both(live, jnp.logical_not(halved)), "y")
-            wire.put(half_refs, key, at_y, both(live, halved), "y")
+            wire.put(refs, key, at_y, both(live, jnp.logical_not(halved)))
+            if (name, j) not in FULL_SIDE:
+                wire.put(half_refs, key, at_y, both(live, halved))
 
     def own(name, j):
         refs = lambda: (piece(name, j, z, y),) * 2
         wire.put(refs, (name, j, "u", 1), at_up, top_end)
         wire.put(refs, (name, j, "d", 1), at_down, low_end)
         over_y(name, j, z, "own", None)
-        if reach > 1:
-            wire.put(refs, (name, j, "u", 2), at_up2, top2)
-            wire.put(refs, (name, j, "d", 2), at_down2, low2)
 
     def forward(name, j, k):
         for way, zz, live, device, ahead, halved in (
@@ -352,14 +371,15 @@
             ("d", z + k, z + k < nz, at_down, low_end, even),
         ):
             when(live, lambda: wire.got(piece(name, j, zz, y), (name, j, way, k)))
-            if reach <= k < nz - 1:
+            if k < nz - 1:
                 wire.put(lambda zz=zz: (piece(name, j, zz, y),) * 2, (name, j, way, k + 1),
                          device, both(live, ahead))
             over_y(name, j, zz, (way, k), live, halved if k == 1 else None)
 
     def side(name, j):
         wire.got(piece(name, j, z, 1 - y), (name, j, "y", "own"))
-        refs = lambda: (piece(name, j, z, 1 - y, 2),) * 2
+        share = 0 if (name, j) in FULL_SIDE else 2
+        refs = lambda: (piece(name, j, z, 1 - y, share),) * 2
         wire.put(refs, (name, j, "side"), at_up, even)
         wire.put(refs, (name, j, "side"), at_down, odd)
 
@@ -370,23 +390,21 @@
             ):
                 key = (name, j, "y", (tag, k))
                 if k == 1:
-                    when(jnp.logical_and(live, halved), lambda: wire.got(
-                        piece(name, j, zz, 1 - y, 1), key))
+                    if (name, j) not in FULL_SIDE:
+                        when(jnp.logical_and(live, halved), lambda: wire.got(
+                            piece(name, j, zz, 1 - y, 1), key))
                     live = jnp.logical_and(live, jnp.logical_not(halved))
                 when(live, lambda: wire.got(piece(name, j, zz, 1 - y), key))
-        wire.got(piece(name, j, z + 1 - 2 * (z % 2), 1 - y, 2), (name, j, "side"))
-
-    order = [("up", 0)] + [("dn", q) for q in range(nq)] + [("up", q) for q in range(1, nq)]
-
-    def next_piece(p):
-        if p < len(order):
-            name, j = order[p]
-            ready((name, j))
-            if name == "dn":
-                wire.got(own_dn(j, 1 - x), ("swap", j))
-            own(name, j)
-
-    next_piece(0)
+        share = 0 if (name, j) in FULL_SIDE else 2
+        wire.got(piece(name, j, z + 1 - 2 * (z % 2), 1 - y, share), (name, j, "side"))
+
+    def send_piece(name, j):
+        ready((name, j))
+        if name == "dn":
+            wire.got(own_dn(j, 1 - x), ("swap", j))
+        own(name, j)
+
+    send_piece("up", 0)
 
     wire.got(st2, "stats")
     short = 16
@@ -410,28 +428,39 @@
     def d_tile(t, n_chunk, h):
         return d_out.at[pl.ds(t * rows + n_chunk * step, step), pl.ds(h * half, half)]
 
-    for n in range(chunks):
+    def send_d(n):
         norm(n)
-        wire.put(lambda n=n: (d_tile(0, n, 0), d_tile(1, n, 0)), ("d_x", n), at_x)
-        wire.put(lambda n=n: (d_tile(0, n, 0), d_tile(0, n, 1)), ("d_core", 0, n), at_core)
-
-    gx[...] = jnp.sum(gacc[...], axis=0, keepdims=True)
-    wire.put(lambda: (gx, gx2), "gain_x", at_x)
-    wire.put(lambda: (inp, inp_v.at[1]), "inp", at_x)
-    for q in range(nq):
-        wire.put(lambda q=q: (
-            pre.at[:, pl.ds(pl.multiple_of((2 * q + 1 - x) * blk, blk), blk)], pre_v.at[1, q]),
-            ("pre", q), at_x)
-
-    def turn(t):
-        def cols_of(i, carry):
-            c = pl.ds(pl.multiple_of(i * blk, blk), blk)
-            for k in range(half // blk):
-                inp_t[pl.ds(k * blk, blk), pl.ds(pl.multiple_of(t * rows + i * blk, blk), blk)] = (
-                    inp_v[t, c, pl.ds(k * blk, blk)].T)
+        wire.put(lambda: (d_tile(0, n, 0), d_tile(1, n, 0)), ("d_x", n), at_x)
+        wire.put(lambda: (d_tile(0, n, 0), d_tile(0, n, 1)), ("d_core", 0, n), at_core)
+
+    def send_x():
+        gx[...] = jnp.sum(gacc[...], axis=0, keepdims=True)
+        wire.put(lambda: (gx, gx2), "gain_x", at_x)
+        for kind, q in X_ORDER:
+            if kind == "inp":
+                tile = pl.ds(q * high, high)
+                wire.put(lambda tile=tile: (inp.at[:, tile], inp_v.at[1, :, tile]),
+                         ("inp", q), at_x)
+            else:
+                wire.put(lambda q=q: (
+                    pre.at[:, pl.ds(pl.multiple_of((2 * q + 1 - x) * blk, blk), blk)],
+                    pre_v.at[1, q]), ("pre", q), at_x)
+
+    def turn(t, r):
+        tile = pl.ds(r * high, high)
+        if t == 0:
+            if r == 0:
+                ready("inp")
+        else:
+            wire.got(inp_v.at[1, :, tile], ("inp", r))
+
+        def rows_of(i, carry):
+            tokens = pl.ds(pl.multiple_of(i * blk, blk), blk)
+            inp_t[tile, pl.ds(pl.multiple_of(t * rows + i * blk, blk), blk)] = (
+                inp_v[t, tokens, tile].T)
             return carry
 
-        lax.fori_loop(0, rows // blk, cols_of, 0)
+        lax.fori_loop(0, rows // blk, rows_of, 0)
 
     def act(t, q):
         def rows_of(i, carry):
@@ -445,12 +474,6 @@
         tile = lambda s: dp.at[pl.ds(t * rows, rows), pl.ds((s * nq + q) * blk, blk)]
         wire.put(lambda: (tile(0), tile(1)), ("dp", t, q), at_core)
 
-    def relay(p, k):
-        forward(*order[p], k)
-        if k == 1:
-            side(*order[p])
-            next_piece(p + 3)
-
     def d_back(n):
         wire.got(d_tile(1, n, 0), ("d_x", n))
         wire.put(lambda: (d_tile(1, n, 0), d_tile(1, n, 1)), ("d_core", 1, n), at_core)
@@ -470,7 +493,9 @@
         wire.got(pre_v.at[1, q], ("pre", q))
         act(1, q)
 
-    def back(r):
+    def back_far(r):
+        arrived("up", r)
+
         def rows_of(i, carry):
             k = pl.ds(pl.multiple_of(i * blk, blk), blk)
             w = up[pl.ds(r * high, high), :]
@@ -478,32 +503,37 @@
             gi_send[r, k, :] = far.astype(bf16)
             return carry
 
-        def rows_own(i, carry):
+        lax.fori_loop(0, rows // blk, rows_of, 0)
+        wire.put(lambda: (gi_send.at[r], gi_got.at[r]), ("gi", r), at_x)
+
+    def back_own(r):
+        def rows_of(i, carry):
             k = pl.ds(pl.multiple_of(i * blk, blk), blk)
             w = up[pl.ds(r * high, high), :]
             gi_own[r, k, :] = mm(dp[k, :], w)
             return carry
 
         lax.fori_loop(0, rows // blk, rows_of, 0)
-        wire.put(lambda: (gi_send.at[r], gi_got.at[r]), ("gi", r), at_x)
-        lax.fori_loop(0, rows // blk, rows_own, 0)
-
-    def grads(q):
+
+    def have_pre(q):
         for t in range(nx):
             wire.got(dp.at[pl.ds(t * rows, rows), pl.ds((nq + q) * blk, blk)], ("dp", t, q))
+
+    def grads(q, r):
         for j in (q, nq + q):
-            for r in range(nq):
-                part[r, j] = lax.dot_general(
-                    inp_t[pl.ds(r * high, high), :], dp[:, pl.ds(j * blk, blk)],
-                    (((1,), (0,)), ((), ())), preferred_element_type=f32)
+            part[r, j] = lax.dot_general(
+                inp_t[pl.ds(r * high, high), :], dp[:, pl.ds(j * blk, blk)],
+                (((1,), (0,)), ((), ())), preferred_element_type=f32)
 
     def goals(q):
         return [divmod(b, ny) for b in (q, nq + q)]
 
-    def first_y(r):
-        return r >= split
+    def first_y(q, r):
+        return (q, r) in Y_FIRST
 
     def to_y(q, r):
+        if not first_y(q, r):
+            return
         for goal, column in goals(q):
             live = y != column
 
@@ -523,13 +553,13 @@
                 slot = chain.at[kind, r, goal, column]
                 key = ("sum", kind, r, goal, column)
                 live = z == at
-                if first_y(r):
+                if first_y(q, r):
                     live = jnp.logical_and(live, y == column)
 
                 @pl.when(live)
                 def _():
                     value = part[r, place(goal, column)]
-                    if first_y(r):
+                    if first_y(q, r):
                         wire.got(y_got.at[r, goal], ("y", r, goal))
                         value = value + y_got[r, goal].astype(f32)
                     if level > 0:
@@ -543,13 +573,13 @@
     def settle(q, r):
         for goal, column in goals(q):
             live = z == goal
-            if first_y(r):
+            if first_y(q, r):
                 live = jnp.logical_and(live, y == column)
 
             @pl.when(live)
             def _():
                 value = part[r, place(goal, column)]
-                if first_y(r):
+                if first_y(q, r):
                     wire.got(y_got.at[r, goal], ("y", r, goal))
                     value = value + y_got[r, goal].astype(f32)
                 for kind in range(2):
@@ -557,40 +587,29 @@
                         slot = chain.at[kind, r, goal, column]
                         wire.got(slot, ("sum", kind, r, goal, column))
                         value = value + slot[...].astype(f32)
-                if first_y(r):
+                if first_y(q, r):
                     gu_out[pl.ds(r * high, high), :] = value * scaled
                 else:
                     acc[r] = value
 
-            if not first_y(r):
+            if not first_y(q, r):
                 away = jnp.logical_and(live, y != column)
 
                 @pl.when(away)
                 def _():
-                    y_send[r, 0] = acc[r].astype(bf16)
+                    tot_send[r] = acc[r].astype(bf16)
 
                 @pl.when(jnp.logical_and(live, y == column))
                 def _():
                     gu_out[pl.ds(r * high, high), :] = acc[r]
 
-                wire.put(lambda: (y_send.at[r, 0], y_got.at[r, 0]), ("y", r), at_y, away)
-
-    split = nq // 2
-    first = list(range(split))
-    later = list(range(split, nq))
-
-    def step_of(rows_set, q, level):
-        for r in rows_set:
-            if level < nz - 1:
-                link(q, r, level)
-            else:
-                settle(q, r)
-
-    def z_step(q, level):
-        step_of(first, q, level)
-
-    def y_step(q, level):
-        step_of(later, q, level)
+                wire.put(lambda: (tot_send.at[r], tot_got.at[r]), ("total", r), at_y, away)
+
+    def sum_step(q, r, level):
+        if level < nz - 1:
+            link(q, r, level)
+        else:
+            settle(q, r)
 
     def gain_over_y():
         wire.got(gx2, "gain_x")
@@ -602,10 +621,6 @@
         gz[z] = gy[...] + gy2[...]
         wire.put(lambda: (gz.at[z], gz.at[z]), ("gain", "u", 1), at_up, top_end)
         wire.put(lambda: (gz.at[z], gz.at[z]), ("gain", "d", 1), at_down, low_end)
-
-    def over_rows(q):
-        for r in later:
-            to_y(q, r)
 
     def gain_relay(k):
         for key, slot, live, device, ahead in (
@@ -616,101 +631,171 @@
                 wire.put(lambda slot=slot: (gz.at[slot], gz.at[slot]), ("gain", key, k + 1),
                          device, both(live, ahead))
 
-    for p in range(1, 3):
-        next_piece(p)
-    relay(0, 1)
-    relay(1, 1)
-    relay(0, 2)
-    relay(2, 1)
+    send_piece("up", 1)
+    send_d(0)
+    for r in range(nq):
+        turn(0, r)
+    send_piece("dn", 0)
+    send_piece("dn", 2)
+    side("up", 0)
+    send_d(1)
+    send_d(2)
+    send_piece("dn", 1)
+    forward("dn", 2, 1)
+    forward("dn", 0, 1)
+    send_d(3)
+    send_x()
+    forward("dn", 2, 2)
+    d_back(1)
+    forward("dn", 0, 2)
     d_back(0)
-    relay(1, 2)
-    relay(2, 2)
-    relay(3, 1)
-    relay(0, 3)
-    relay(1, 3)
-    relay(2, 3)
-    d_back(1)
-    ready("inp")
-    turn(0)
+    side("dn", 2)
+    side("dn", 1)
+    side("dn", 0)
+    send_piece("up", 3)
+    forward("dn", 0, 3)
+    send_piece("dn", 3)
+    forward("dn", 1, 1)
+    act_own(0)
+    send_piece("up", 2)
+    forward("dn", 3, 1)
     d_back(2)
+    side("up", 1)
+    forward("up", 0, 1)
     d_back(3)
     gain_over_y()
-    relay(4, 1)
-    act_own(0)
-    relay(3, 2)
-    relay(4, 2)
-    relay(5, 1)
-    wire.got(inp_v.at[1], "inp")
-    turn(1)
+    forward("dn", 2, 3)
+    side("up", 3)
+    act_far(0)
+    have_pre(0)
+    turn(1, 0)
+    grads(0, 0)
+    forward("dn", 1, 2)
+    sum_step(0, 0, 0)
+    turn(1, 2)
+    forward("dn", 3, 2)
+    forward("up", 2, 1)
+    act_own(2)
+    side("dn", 3)
+    gain_over_z()
+    grads(0, 2)
+    sum_step(0, 2, 0)
+    forward("up", 0, 2)
+    forward("up", 1, 1)
+    side("up", 2)
+    act_far(2)
+    have_pre(2)
+    grads(2, 0)
+    sum_step(2, 0, 0)
+    forward("dn", 1, 3)
+    turn(1, 1)
+    sum_step(0, 2, 1)
+    forward("dn", 3, 3)
+    grads(0, 1)
+    grads(2, 1)
+    sum_step(2, 1, 0)
+    sum_step(2, 0, 1)
+    forward("up", 2, 2)
+    grads(2, 2)
+    sum_step(0, 1, 0)
     act_own(1)
-    relay(6, 1)
-    gain_over_z()
-    act_far(0)
-    grads(0)
-    relay(3, 3)
-    z_step(0, 0)
+    forward("up", 3, 1)
     act_far(1)
-    relay(4, 3)
-    grads(1)
-    z_step(1, 0)
-    act_own(2)
-    act_far(2)
-    relay(5, 2)
-    relay(6, 2)
-    relay(7, 1)
-    grads(2)
+    act_own(3)
+    have_pre(1)
+    forward("up", 0, 3)
+    grads(1, 1)
+    forward("up", 1, 2)
+    sum_step(0, 0, 1)
+    sum_step(2, 1, 1)
     gain_relay(1)
-    z_step(2, 0)
-    relay(5, 3)
-    z_step(0, 1)
-    relay(6, 3)
-    act_own(3)
+    sum_step(1, 1, 0)
+    grads(1, 2)
+    to_y(2, 2)
+    sum_step(0, 1, 1)
     act_far(3)
-    grads(3)
-    over_rows(3)
-    over_rows(2)
-    over_rows(0)
-    z_step(0, 2)
-    z_step(3, 0)
-    arrived("up", 1)
-    back(1)
-    over_rows(1)
-    relay(7, 2)
+    grads(1, 0)
+    forward("up", 2, 3)
+    have_pre(3)
+    sum_step(1, 2, 0)
+    sum_step(2, 0, 2)
+    grads(3, 2)
+    grads(3, 1)
+    forward("up", 3, 2)
+    sum_step(3, 1, 0)
+    turn(1, 3)
+    grads(0, 3)
+    sum_step(3, 2, 0)
+    sum_step(1, 0, 0)
+    forward("up", 1, 3)
+    grads(3, 0)
+    sum_step(1, 1, 1)
+    grads(3, 3)
+    to_y(3, 0)
+    grads(1, 3)
+    sum_step(2, 2, 0)
+    sum_step(1, 2, 1)
+    grads(2, 3)
+    sum_step(0, 0, 2)
+    back_far(2)
+    to_y(2, 3)
     gain_relay(2)
-    z_step(1, 1)
-    relay(7, 3)
-    y_step(3, 0)
-    y_step(2, 0)
-    arrived("up", 2)
-    back(2)
-    y_step(0, 0)
-    z_step(2, 1)
-    y_step(1, 0)
-    z_step(2, 2)
-    z_step(3, 1)
-    z_step(1, 2)
-    z_step(1, 3)
-    z_step(3, 2)
-    z_step(3, 3)
-    y_step(3, 1)
+    to_y(3, 3)
+    sum_step(0, 2, 2)
+    back_own(2)
+    sum_step(3, 1, 1)
+    back_far(0)
+    back_far(1)
+    sum_step(1, 2, 2)
+    sum_step(2, 1, 2)
+    sum_step(3, 1, 2)
+    sum_step(1, 1, 2)
+    sum_step(3, 2, 1)
+    to_y(1, 3)
+    to_y(0, 3)
+    sum_step(1, 0, 1)
+    sum_step(2, 3, 0)
+    sum_step(3, 0, 0)
+    sum_step(2, 2, 1)
+    sum_step(3, 3, 0)
+    sum_step(3, 2, 2)
+    forward("up", 3, 3)
+    sum_step(1, 3, 0)
+    sum_step(2, 1, 3)
+    sum_step(0, 3, 0)
+    sum_step(3, 2, 3)
+    sum_step(3, 1, 3)
+    sum_step(2, 0, 3)
+    sum_step(1, 1, 3)
     gain_relay(3)
-    y_step(2, 1)
-    arrived("up", 0)
-    back(0)
-    arrived("up", 3)
-    back(3)
-    z_step(2, 3)
-    y_step(1, 1)
-    y_step(0, 1)
-    y_step(3, 2)
-    y_step(0, 2)
-    z_step(0, 3)
-    y_step(1, 2)
-    y_step(2, 2)
-    y_step(2, 3)
-    y_step(3, 3)
-    y_step(0, 3)
-    y_step(1, 3)
+    back_own(1)
+    sum_step(0, 2, 3)
+    sum_step(0, 1, 2)
+    sum_step(3, 0, 1)
+    sum_step(1, 0, 2)
+    back_far(3)
+    sum_step(2, 3, 1)
+    back_own(0)
+    sum_step(3, 3, 1)
+    sum_step(2, 2, 3)
+    sum_step(3, 0, 3)
+    sum_step(0, 3, 1)
+    sum_step(1, 3, 1)
+    sum_step(3, 0, 2)
+    back_own(3)
+    sum_step(1, 2, 3)
+    sum_step(3, 3, 3)
+    sum_step(0, 0, 3)
+    sum_step(0, 1, 3)
+    sum_step(2, 2, 2)
+    sum_step(1, 0, 3)
+    sum_step(3, 3, 2)
+    sum_step(2, 3, 2)
+    sum_step(2, 3, 3)
+    sum_step(1, 3, 2)
+    sum_step(1, 3, 3)
+    sum_step(0, 3, 3)
+    sum_step(0, 3, 2)
     total = gz[0]
     for k in range(1, nz):
         total = total + gz[k]
@@ -718,10 +803,15 @@
     for r in range(nq):
         wire.got(gi_got.at[r], ("gi", r))
         gi_out[:, pl.ds(r * high, high)] = (gi_own[r] + gi_got[r].astype(f32)).astype(bf16)
-    for r in first:
-        wire.got(y_got.at[r, 0], ("y", r))
+    stage = lax.rem(z * ny + y, nq)
+    for r in range(nq):
         tile = pl.ds(r * high, high)
-        gu_out[tile, :] = (gu_out[tile, :] + y_got[r, 0].astype(f32)) * scaled
+        for q in range(nq):
+            if not first_y(q, r):
+                @pl.when(stage == q)
+                def _():
+                    wire.got(tot_got.at[r], ("total", r))
+                    gu_out[tile, :] = (gu_out[tile, :] + tot_got[r].astype(f32)) * scaled
     wire.drain()
 
 
@@ -746,12 +836,12 @@
         v((nq, rows, high), f32), v((nq, rows, high), bf16), v((nq, rows, high), bf16),
         v((2, nq, nz, ny, high, blk), bf16),
         v((nq, nz, high, blk), bf16), v((nq, nz, high, blk), bf16),
-        v((nq // 2, high, blk), f32),
+        v((nq, high, blk), bf16), v((nq, high, blk), bf16), v((nq, high, blk), f32),
         v((8, half), f32),
         v((1, half), f32), v((1, half), f32), v((1, half), f32), v((1, half), f32),
         v((nz, 1, half), f32),
         pltpu.SemaphoreType.DMA((3 + 3 * nq + 1,)),
-        pltpu.SemaphoreType.DMA((SEMS,)), pltpu.SemaphoreType.DMA((SEMS,)),
+        pltpu.SemaphoreType.DMA((SENDS,)), pltpu.SemaphoreType.DMA((RECVS,)),
     ]
     flops = 3 * 2 * nx * rows * 2 * half * hid
     shapes = ((rows, half), bf16), ((half, blk), f32), ((1, half), f32)
@@ -793,7 +883,8 @@
 
     def solve(*args):
         up, down = args[4].shape, args[5].shape
-        if tp == 2 and fs % 8 == 0 and up[1] // fs % 256 == 0 and down[1] // fs % 128 == 0:
+        whole = up[1] // fs % 128 == 0 and down[1] // fs % 128 == 0
+        if tp == 2 and fs == 4 * PLAN_STEPS and whole:
             return jax.shard_map(
                 in_kernel, mesh=mesh, in_specs=placed, out_specs=out_specs, check_vma=False
             )(*args)

time: 137 us -> 125 us (0.912)
  Pallas kernels: 134 us -> 121 us
    pallas_call x1, Pallas kernels: 134 us -> 121 us  [kernel_step(): pl.pallas_call(functools.partial(fused, nz, ny), out_shape=tuple((v(*shap...]
where the time goes in v2:
time: 125 us
  Pallas kernels  121 us (97%)
  local copies, waits for them, and re-layouts  2.54 us (2%)
    pallas_call x1, Pallas kernels, kernel_step(): pl.pallas_call(functools.partial(fused, nz, ny), out_shape=tuple((v(*shap...  121 us
    unnamed x3, local copies, waits for them, and re-layouts  2.54 us

profile of v2, /device:TPU:0, one launch (start us, length us, event | category | flops | bytes accessed | tf_op | source)
XLA Modules:
  0.0 124.5 jit_solution(16691904537383323752)
XLA Ops:
  0.6 121.3 %layer_backward.1 = (bf16[512,1024]{1,0:T(8,128)(2,1)S(1)}, f32[1024,256]{1,0:T(8,128)S(1)}, f32[1,1024]{1,0:T(1,128)S(1)}) custom-call(bf16[512,1024]{1,0:T(8,128)(2,1)} %inp.1, bf16[512,2048]{1,0:T(8,128)(2,1)} %pre.1, bf16[512,1024]{1,0:T(8,128)(2,1)} %nrm.1, f32[1,1024]{1,0:T(1,128)} %bitcast.5, bf16[1024,256]{1,0:T(8,128)(2,1)} %wu.1, ...), custom_call_target="tpu_custom_call" | custom-call | flops 12884901888 | bytes 16777216 | tf_op jit(solution)/shard_map/layer_backward/pallas_call | solution.py:848
  122.0 1.0 copy.13
  122.9 0.6 copy.15
  123.5 1.0 copy.14

commit v3 on v2

--- a/solution.py
+++ b/solution.py
@@ -1,4 +1,5 @@
 import functools
+import math
 
 import jax
 import jax.numpy as jnp
@@ -10,8 +11,8 @@
 
 norm_eps = 1e-06
 MESH = pl.DeviceIdType.MESH
-SENDS = 170
-RECVS = 160
+SENDS = 93
+RECVS = 157
 PLAN_STEPS = 4
 FULL_SIDE = ()
 Y_FIRST = ((0, 3), (1, 3), (2, 2), (2, 3), (3, 0), (3, 3))
@@ -181,7 +182,7 @@
 class Wire:
     def __init__(self, send, recv, other, nz):
         self.send, self.recv, self.other, self.nz = send, recv, other, nz
-        self.sent, self.came, self.pending = {}, {}, []
+        self.sent, self.came, self.pending, self.groups = {}, {}, [], {}
 
     def arrives(self, key):
         *head, way, k = key if isinstance(key, tuple) else (key, None, None)
@@ -206,8 +207,8 @@
         assert index < sems.shape[0], "semaphores"
         return sems.at[index]
 
-    def put(self, refs, key, device, live=None):
-        out = self.at(self.send, self.sent, self.departs(key))
+    def put(self, refs, key, device, live=None, group=None):
+        out = self.at(self.send, self.sent, group or self.departs(key))
         arrival = self.at(self.recv, self.came, self.arrives(key))
 
         def copy():
@@ -218,7 +219,12 @@
             )
 
         when(live, lambda: copy().start())
-        self.pending.append((copy, live))
+        if group is None:
+            self.pending.append((copy, live))
+        else:
+            source = refs()[0]
+            size = math.prod(source.shape) * source.dtype.itemsize
+            self.groups.setdefault(group, [out, live, 0])[2] += size
 
     def got(self, ref, key):
         pltpu.make_async_remote_copy(
@@ -227,10 +233,15 @@
             device_id=self.other, device_id_type=MESH,
         ).wait_recv()
 
-    def drain(self):
+    def drain(self, like):
         for copy, live in self.pending:
             when(live, lambda: copy().wait_send())
-        self.pending = []
+        for out, live, size in self.groups.values():
+            ref = like.at[pl.ds(0, size // (like.shape[1] * like.dtype.itemsize)), :]
+            when(live, lambda: pltpu.make_async_remote_copy(
+                src_ref=ref, dst_ref=ref, send_sem=out, recv_sem=self.recv.at[0],
+                device_id=self.other, device_id_type=MESH,
+            ).wait_send())
 
 
 def when(live, body):
@@ -334,7 +345,7 @@
 
     wire.put(lambda: (st, st2), "stats", at_core)
     for q in range(nq):
-        wire.put(lambda q=q: (wd.at[q, 1 - x], own_dn(q, x)), ("swap", q), at_x)
+        wire.put(lambda q=q: (wd.at[q, 1 - x], own_dn(q, x)), ("swap", q), at_x, None, "swap")
 
 
     def piece(name, j, zz, yy, part_of=0):
@@ -353,7 +364,7 @@
         half_refs = lambda: (piece(name, j, zz, y, 1),) * 2
         key = (name, j, "y", tag)
         if halved is None:
-            wire.put(refs, key, at_y, live)
+            wire.put(refs, key, at_y, live, ("y", tag))
         else:
             wire.put(refs, key, at_y, both(live, jnp.logical_not(halved)))
             if (name, j) not in FULL_SIDE:
@@ -361,8 +372,8 @@
 
     def own(name, j):
         refs = lambda: (piece(name, j, z, y),) * 2
-        wire.put(refs, (name, j, "u", 1), at_up, top_end)
-        wire.put(refs, (name, j, "d", 1), at_down, low_end)
+        wire.put(refs, (name, j, "u", 1), at_up, top_end, "own_u")
+        wire.put(refs, (name, j, "d", 1), at_down, low_end, "own_d")
         over_y(name, j, z, "own", None)
 
     def forward(name, j, k):
@@ -373,7 +384,7 @@
             when(live, lambda: wire.got(piece(name, j, zz, y), (name, j, way, k)))
             if k < nz - 1:
                 wire.put(lambda zz=zz: (piece(name, j, zz, y),) * 2, (name, j, way, k + 1),
-                         device, both(live, ahead))
+                         device, both(live, ahead), ("z", way, k))
             over_y(name, j, zz, (way, k), live, halved if k == 1 else None)
 
     def side(name, j):
@@ -430,8 +441,8 @@
 
     def send_d(n):
         norm(n)
-        wire.put(lambda: (d_tile(0, n, 0), d_tile(1, n, 0)), ("d_x", n), at_x)
-        wire.put(lambda: (d_tile(0, n, 0), d_tile(0, n, 1)), ("d_core", 0, n), at_core)
+        wire.put(lambda: (d_tile(0, n, 0), d_tile(1, n, 0)), ("d_x", n), at_x, None, "d_x")
+        wire.put(lambda: (d_tile(0, n, 0), d_tile(0, n, 1)), ("d_core", 0, n), at_core, None, "d_core")
 
     def send_x():
         gx[...] = jnp.sum(gacc[...], axis=0, keepdims=True)
@@ -440,11 +451,11 @@
             if kind == "inp":
                 tile = pl.ds(q * high, high)
                 wire.put(lambda tile=tile: (inp.at[:, tile], inp_v.at[1, :, tile]),
-                         ("inp", q), at_x)
+                         ("inp", q), at_x, None, "inp")
             else:
                 wire.put(lambda q=q: (
                     pre.at[:, pl.ds(pl.multiple_of((2 * q + 1 - x) * blk, blk), blk)],
-                    pre_v.at[1, q]), ("pre", q), at_x)
+                    pre_v.at[1, q]), ("pre", q), at_x, None, "pre")
 
     def turn(t, r):
         tile = pl.ds(r * high, high)
@@ -472,11 +483,11 @@
 
         lax.fori_loop(0, rows // blk, rows_of, 0)
         tile = lambda s: dp.at[pl.ds(t * rows, rows), pl.ds((s * nq + q) * blk, blk)]
-        wire.put(lambda: (tile(0), tile(1)), ("dp", t, q), at_core)
+        wire.put(lambda: (tile(0), tile(1)), ("dp", t, q), at_core, None, "dp")
 
     def d_back(n):
         wire.got(d_tile(1, n, 0), ("d_x", n))
-        wire.put(lambda: (d_tile(1, n, 0), d_tile(1, n, 1)), ("d_core", 1, n), at_core)
+        wire.put(lambda: (d_tile(1, n, 0), d_tile(1, n, 1)), ("d_core", 1, n), at_core, None, "d_core")
 
     def act_own(q):
         if q == 0:
@@ -504,7 +515,7 @@
             return carry
 
         lax.fori_loop(0, rows // blk, rows_of, 0)
-        wire.put(lambda: (gi_send.at[r], gi_got.at[r]), ("gi", r), at_x)
+        wire.put(lambda: (gi_send.at[r], gi_got.at[r]), ("gi", r), at_x, None, "gi")
 
     def back_own(r):
         def rows_of(i, carry):
@@ -812,7 +823,7 @@
                 def _():
                     wire.got(tot_got.at[r], ("total", r))
                     gu_out[tile, :] = (gu_out[tile, :] + tot_got[r].astype(f32)) * scaled
-    wire.drain()
+    wire.drain(dn)
 
 
 def kernel_step(fs, tp, inputs, hidden_pre, norm_input, out_gain, w_up, w_down, cotangent):
@@ -860,8 +871,27 @@
         inputs, hidden_pre, norm_input, out_gain.reshape(1, half), w_up,
         w_down.reshape(nq, nx, blk, cols), cotangent,
     )
-    grad_input, grad_up, grad_gain = results
+    results = [pltpu.with_memory_space_constraint(a, pltpu.VMEM) for a in results]
+    grad_input, grad_up, grad_gain = pl.pallas_call(
+        deliver,
+        out_shape=tuple(jax.ShapeDtypeStruct(*shape) for shape in shapes),
+        in_specs=[pl.BlockSpec(memory_space=pltpu.VMEM)] * 3,
+        out_specs=(pl.BlockSpec(memory_space=pl.ANY),) * 3,
+        scratch_shapes=[pltpu.SemaphoreType.DMA((3,))],
+        name="deliver",
+    )(*results)
     return grad_input, grad_up, grad_gain.reshape(half)
+
+
+def deliver(*refs):
+    *refs, sems = refs
+    copies = [
+        pltpu.make_async_copy(refs[i], refs[3 + i], sems.at[i]) for i in range(3)
+    ]
+    for copy in copies:
+        copy.start()
+    for copy in copies:
+        copy.wait()
 
 
 def in_kernel(*args):

time: 125 us -> 123 us (0.984)
  local copies, waits for them, and re-layouts: 2.54 us -> 0 us
    unnamed x3 -> x0, local copies, waits for them, and re-layouts: 2.54 us -> none
    pallas_call x0 -> x1, Pallas kernels: none -> 1.35 us  [kernel_step(): pl.pallas_call(deliver, out_shape=tuple((jax.ShapeDtypeStruct(*shape) for...]
where the time goes in v3:
time: 123 us
  Pallas kernels  122 us (99%)
    pallas_call x1, Pallas kernels, kernel_step(): pl.pallas_call(functools.partial(fused, nz, ny), out_shape=tuple((v(*shap...  121 us

profile of v3, /device:TPU:0, one launch (start us, length us, event | category | flops | bytes accessed | tf_op | source)
XLA Modules:
  0.0 122.7 jit_solution(8613260407582089987)
XLA Ops:
  0.6 120.5 %layer_backward.1 = (bf16[512,1024]{1,0:T(8,128)(2,1)S(1)}, f32[1024,256]{1,0:T(8,128)S(1)}, f32[1,1024]{1,0:T(1,128)S(1)}) custom-call(bf16[512,1024]{1,0:T(8,128)(2,1)} %inp.1, bf16[512,2048]{1,0:T(8,128)(2,1)} %pre.1, bf16[512,1024]{1,0:T(8,128)(2,1)} %nrm.1, f32[1,1024]{1,0:T(1,128)} %bitcast.4, bf16[1024,256]{1,0:T(8,128)(2,1)} %wu.1, ...), custom_call_target="tpu_custom_call" | custom-call | flops 12884901888 | bytes 16777216 | tf_op jit(solution)/shard_map/layer_backward/pallas_call | solution.py:859
  121.1 1.3 %deliver.1 = (bf16[512,1024]{1,0:T(8,128)(2,1)}, f32[1024,256]{1,0:T(8,128)}, f32[1,1024]{1,0:T(1,128)}) custom-call(bf16[512,1024]{1,0:T(8,128)(2,1)S(1)} %get-tuple-element.9.refs_0_, f32[1024,256]{1,0:T(8,128)S(1)} %get-tuple-element.10.refs_1_, f32[1,1024]{1,0:T(1,128)S(1)} %get-tuple-element.11.refs_2_), custom_call_target="tpu_custom_call" | custom-call | tf_op jit(solution)/shard_map/deliver/pallas_call | solution.py:875

commit v4 on v3

--- a/solution.py
+++ b/solution.py
@@ -11,12 +11,12 @@
 
 norm_eps = 1e-06
 MESH = pl.DeviceIdType.MESH
-SENDS = 93
-RECVS = 157
+SENDS = 99
+RECVS = 163
 PLAN_STEPS = 4
-FULL_SIDE = ()
-Y_FIRST = ((0, 3), (1, 3), (2, 2), (2, 3), (3, 0), (3, 3))
-X_ORDER = (("pre", 0), ("inp", 0), ("inp", 2), ("pre", 2), ("inp", 1), ("pre", 1), ("pre", 3), ("inp", 3))
+FULL_SIDE = (("dn", 2),)
+Y_FIRST = ((0, 1), (0, 3), (1, 0), (1, 3), (2, 2), (2, 3), (3, 1), (3, 3))
+X_ORDER = (("pre", 0), ("pre", 3), ("inp", 2), ("inp", 0), ("pre", 1), ("inp", 1), ("pre", 2), ("inp", 3))
 
 
 def trade(x, axis, mask):
@@ -642,171 +642,173 @@
                 wire.put(lambda slot=slot: (gz.at[slot], gz.at[slot]), ("gain", key, k + 1),
                          device, both(live, ahead))
 
-    send_piece("up", 1)
-    send_d(0)
     for r in range(nq):
         turn(0, r)
+    send_d(0)
+    send_piece("up", 1)
     send_piece("dn", 0)
-    send_piece("dn", 2)
-    side("up", 0)
+    send_piece("up", 2)
+    send_piece("dn", 3)
     send_d(1)
     send_d(2)
     send_piece("dn", 1)
+    send_d(3)
+    forward("dn", 0, 1)
+    send_x()
+    forward("dn", 3, 1)
+    forward("dn", 1, 1)
+    side("dn", 0)
+    forward("dn", 0, 2)
+    forward("dn", 3, 2)
+    send_piece("dn", 2)
+    d_back(0)
+    forward("up", 0, 1)
+    forward("dn", 0, 3)
+    forward("dn", 3, 3)
+    side("dn", 3)
     forward("dn", 2, 1)
-    forward("dn", 0, 1)
-    send_d(3)
-    send_x()
-    forward("dn", 2, 2)
+    forward("dn", 1, 2)
+    send_piece("up", 3)
+    forward("up", 0, 2)
+    forward("up", 2, 1)
+    d_back(2)
+    side("dn", 1)
+    act_own(0)
     d_back(1)
-    forward("dn", 0, 2)
-    d_back(0)
-    side("dn", 2)
-    side("dn", 1)
-    side("dn", 0)
-    send_piece("up", 3)
-    forward("dn", 0, 3)
-    send_piece("dn", 3)
-    forward("dn", 1, 1)
-    act_own(0)
-    send_piece("up", 2)
-    forward("dn", 3, 1)
-    d_back(2)
-    side("up", 1)
-    forward("up", 0, 1)
+    side("up", 2)
+    act_own(3)
     d_back(3)
     gain_over_y()
-    forward("dn", 2, 3)
-    side("up", 3)
+    forward("dn", 2, 2)
+    forward("up", 1, 1)
+    side("up", 1)
     act_far(0)
+    side("dn", 2)
+    act_far(3)
+    forward("dn", 1, 3)
+    turn(1, 2)
+    have_pre(3)
+    grads(3, 2)
+    side("up", 0)
+    sum_step(3, 2, 0)
+    forward("up", 3, 1)
+    gain_over_z()
     have_pre(0)
     turn(1, 0)
     grads(0, 0)
-    forward("dn", 1, 2)
+    sum_step(3, 2, 1)
+    forward("up", 0, 3)
     sum_step(0, 0, 0)
-    turn(1, 2)
-    forward("dn", 3, 2)
-    forward("up", 2, 1)
+    grads(3, 0)
+    grads(0, 2)
+    forward("up", 2, 2)
+    act_own(1)
+    sum_step(3, 0, 0)
+    sum_step(0, 2, 0)
+    sum_step(3, 2, 2)
+    forward("dn", 2, 3)
+    sum_step(0, 0, 1)
+    act_far(1)
+    have_pre(1)
+    forward("up", 1, 2)
+    turn(1, 1)
+    grads(1, 2)
+    side("up", 3)
+    grads(1, 0)
+    sum_step(3, 0, 1)
+    grads(3, 1)
+    grads(0, 1)
+    to_y(0, 1)
+    to_y(1, 0)
+    grads(1, 1)
+    gain_relay(1)
+    sum_step(1, 2, 0)
     act_own(2)
-    side("dn", 3)
-    gain_over_z()
-    grads(0, 2)
-    sum_step(0, 2, 0)
-    forward("up", 0, 2)
-    forward("up", 1, 1)
-    side("up", 2)
+    sum_step(0, 2, 1)
+    sum_step(1, 1, 0)
     act_far(2)
+    forward("up", 3, 2)
+    sum_step(3, 0, 2)
     have_pre(2)
+    grads(2, 1)
     grads(2, 0)
     sum_step(2, 0, 0)
-    forward("dn", 1, 3)
-    turn(1, 1)
-    sum_step(0, 2, 1)
-    forward("dn", 3, 3)
-    grads(0, 1)
-    grads(2, 1)
+    forward("up", 2, 3)
+    turn(1, 3)
+    grads(2, 2)
+    grads(0, 3)
+    grads(1, 3)
+    grads(3, 3)
+    to_y(3, 3)
+    sum_step(1, 1, 1)
     sum_step(2, 1, 0)
-    sum_step(2, 0, 1)
-    forward("up", 2, 2)
-    grads(2, 2)
     sum_step(0, 1, 0)
-    act_own(1)
-    forward("up", 3, 1)
-    act_far(1)
-    act_own(3)
-    have_pre(1)
-    forward("up", 0, 3)
-    grads(1, 1)
-    forward("up", 1, 2)
-    sum_step(0, 0, 1)
-    sum_step(2, 1, 1)
-    gain_relay(1)
-    sum_step(1, 1, 0)
-    grads(1, 2)
-    to_y(2, 2)
-    sum_step(0, 1, 1)
-    act_far(3)
-    grads(1, 0)
-    forward("up", 2, 3)
-    have_pre(3)
-    sum_step(1, 2, 0)
-    sum_step(2, 0, 2)
-    grads(3, 2)
-    grads(3, 1)
-    forward("up", 3, 2)
-    sum_step(3, 1, 0)
-    turn(1, 3)
-    grads(0, 3)
-    sum_step(3, 2, 0)
-    sum_step(1, 0, 0)
-    forward("up", 1, 3)
-    grads(3, 0)
-    sum_step(1, 1, 1)
-    grads(3, 3)
-    to_y(3, 0)
-    grads(1, 3)
-    sum_step(2, 2, 0)
-    sum_step(1, 2, 1)
     grads(2, 3)
     sum_step(0, 0, 2)
+    to_y(1, 3)
+    to_y(2, 2)
+    to_y(2, 3)
+    sum_step(3, 3, 0)
+    sum_step(1, 2, 1)
+    gain_relay(2)
+    to_y(3, 1)
+    sum_step(2, 0, 1)
+    forward("up", 1, 3)
+    to_y(0, 3)
     back_far(2)
-    to_y(2, 3)
-    gain_relay(2)
-    to_y(3, 3)
+    back_far(0)
+    forward("up", 3, 3)
+    sum_step(1, 2, 2)
+    back_own(0)
+    sum_step(2, 1, 1)
+    sum_step(1, 3, 0)
+    sum_step(2, 2, 0)
+    sum_step(3, 2, 3)
+    sum_step(3, 1, 0)
+    sum_step(1, 0, 0)
+    back_own(2)
+    sum_step(0, 1, 1)
+    sum_step(0, 0, 3)
+    sum_step(2, 3, 0)
+    sum_step(2, 0, 2)
+    sum_step(3, 0, 3)
+    back_far(1)
+    sum_step(1, 1, 2)
+    sum_step(1, 2, 3)
+    sum_step(1, 3, 1)
+    sum_step(2, 2, 1)
+    gain_relay(3)
+    sum_step(0, 3, 0)
+    back_far(3)
+    sum_step(0, 1, 2)
+    sum_step(3, 3, 1)
+    sum_step(2, 1, 2)
+    sum_step(2, 3, 1)
+    back_own(1)
     sum_step(0, 2, 2)
-    back_own(2)
+    sum_step(1, 1, 3)
+    sum_step(2, 2, 3)
+    sum_step(2, 1, 3)
+    back_own(3)
+    sum_step(2, 2, 2)
     sum_step(3, 1, 1)
-    back_far(0)
-    back_far(1)
-    sum_step(1, 2, 2)
-    sum_step(2, 1, 2)
+    sum_step(2, 0, 3)
+    sum_step(0, 3, 1)
+    sum_step(3, 3, 3)
+    sum_step(1, 3, 2)
+    sum_step(2, 3, 3)
+    sum_step(0, 2, 3)
+    sum_step(1, 0, 1)
+    sum_step(2, 3, 2)
+    sum_step(1, 0, 2)
+    sum_step(3, 3, 2)
     sum_step(3, 1, 2)
-    sum_step(1, 1, 2)
-    sum_step(3, 2, 1)
-    to_y(1, 3)
-    to_y(0, 3)
-    sum_step(1, 0, 1)
-    sum_step(2, 3, 0)
-    sum_step(3, 0, 0)
-    sum_step(2, 2, 1)
-    sum_step(3, 3, 0)
-    sum_step(3, 2, 2)
-    forward("up", 3, 3)
-    sum_step(1, 3, 0)
-    sum_step(2, 1, 3)
-    sum_step(0, 3, 0)
-    sum_step(3, 2, 3)
+    sum_step(0, 3, 2)
+    sum_step(0, 1, 3)
+    sum_step(1, 3, 3)
     sum_step(3, 1, 3)
-    sum_step(2, 0, 3)
-    sum_step(1, 1, 3)
-    gain_relay(3)
-    back_own(1)
-    sum_step(0, 2, 3)
-    sum_step(0, 1, 2)
-    sum_step(3, 0, 1)
-    sum_step(1, 0, 2)
-    back_far(3)
-    sum_step(2, 3, 1)
-    back_own(0)
-    sum_step(3, 3, 1)
-    sum_step(2, 2, 3)
-    sum_step(3, 0, 3)
-    sum_step(0, 3, 1)
-    sum_step(1, 3, 1)
-    sum_step(3, 0, 2)
-    back_own(3)
-    sum_step(1, 2, 3)
-    sum_step(3, 3, 3)
-    sum_step(0, 0, 3)
-    sum_step(0, 1, 3)
-    sum_step(2, 2, 2)
+    sum_step(0, 3, 3)
     sum_step(1, 0, 3)
-    sum_step(3, 3, 2)
-    sum_step(2, 3, 2)
-    sum_step(2, 3, 3)
-    sum_step(1, 3, 2)
-    sum_step(1, 3, 3)
-    sum_step(0, 3, 3)
-    sum_step(0, 3, 2)
     total = gz[0]
     for k in range(1, nz):
         total = total + gz[k]

time: 123 us -> 126 us (1.024)
  Pallas kernels: 122 us -> 125 us
    pallas_call x1, Pallas kernels: 121 us -> 123 us  [kernel_step(): pl.pallas_call(functools.partial(fused, nz, ny), out_shape=tuple((v(*shap...]
where the time goes in v4:
time: 126 us; the launch traced here: 125 us
  Pallas kernels  125 us (99%)
    pallas_call x1, Pallas kernels, kernel_step(): pl.pallas_call(functools.partial(fused, nz, ny), out_shape=tuple((v(*shap...  123 us

profile of v4, /device:TPU:0, one launch (start us, length us, event | category | flops | bytes accessed | tf_op | source)
XLA Modules:
  0.0 125.4 jit_solution(13588403598873759125)
XLA Ops:
  0.6 123.3 %layer_backward.1 = (bf16[512,1024]{1,0:T(8,128)(2,1)S(1)}, f32[1024,256]{1,0:T(8,128)S(1)}, f32[1,1024]{1,0:T(1,128)S(1)}) custom-call(bf16[512,1024]{1,0:T(8,128)(2,1)} %inp.1, bf16[512,2048]{1,0:T(8,128)(2,1)} %pre.1, bf16[512,1024]{1,0:T(8,128)(2,1)} %nrm.1, f32[1,1024]{1,0:T(1,128)} %bitcast.4, bf16[1024,256]{1,0:T(8,128)(2,1)} %wu.1, ...), custom_call_target="tpu_custom_call" | custom-call | flops 12884901888 | bytes 16777216 | tf_op jit(solution)/shard_map/layer_backward/pallas_call | solution.py:861
  123.9 1.3 %deliver.1 = (bf16[512,1024]{1,0:T(8,128)(2,1)}, f32[1024,256]{1,0:T(8,128)}, f32[1,1024]{1,0:T(1,128)}) custom-call(bf16[512,1024]{1,0:T(8,128)(2,1)S(1)} %get-tuple-element.9.refs_0_, f32[1024,256]{1,0:T(8,128)S(1)} %get-tuple-element.10.refs_1_, f32[1,1024]{1,0:T(1,128)S(1)} %get-tuple-element.11.refs_2_), custom_call_target="tpu_custom_call" | custom-call | tf_op jit(solution)/shard_map/deliver/pallas_call | solution.py:877
